TPU v7x, 32 devices: a whole 2x2x4 slice. The times are simulated.
32 devices in a mesh: fs: 8 (over z, x), tp: 4 (over y, core).
Axes of the slice: x: 2, y: 2, z: 4, core: 2. Of those that a mesh axis runs over, the one named last changes fastest.
Arguments:
- tokens: bfloat16 [4096, 2048], P(('fs', 'tp')), may hold values from -6 to 6
- norm_gain: float32 [2048], replicated, may hold values from 0.1 to 1.9
- up_weight: bfloat16 [2048, 8192], P('fs', 'tp'), may hold values from -0.125 to 0.125
- down_weight: bfloat16 [8192, 2048], P('tp', 'fs'), may hold values from -0.0625 to 0.0625
Outputs:
- mixed: bfloat16 [4096, 2048], P(('fs', 'tp'))
All inputs are finite; a program needn't handle non-finite values.
Results may differ from a plain program's by a relative error of at most 0.013.
Values may be sent and summed in bfloat16 or wider, within the bound.
A program may use at most 64 MiB of HBM per device.

v0:
```python
import functools
import math

import jax
import jax.numpy as jnp
from jax import lax
from jax.experimental import pallas as pl
from jax.experimental.pallas import tpu as pltpu
from jax.sharding import PartitionSpec as P

epsilon = 1e-06
MESH = pl.DeviceIdType.MESH
H = 4
f32, bf16 = jnp.float32, jnp.bfloat16


def plain(tokens, norm_gain, up_weight, down_weight):
    values = tokens.astype(f32)
    mean_square = jnp.mean(values * values, axis=-1, keepdims=True)
    normed = (values * lax.rsqrt(mean_square + epsilon) * norm_gain).astype(bf16)
    up_whole = lax.all_gather(up_weight, "fs", axis=0, tiled=True)
    rows = lax.all_gather(normed, "tp", axis=0, tiled=True)
    preact = jnp.dot(rows, up_whole, preferred_element_type=f32)
    hidden = jnp.square(jnp.maximum(preact, 0.0)).astype(bf16)
    down_whole = lax.all_gather(down_weight, "fs", axis=1, tiled=True)
    partial_value = jnp.dot(hidden, down_whole, preferred_element_type=f32).astype(bf16)
    return lax.psum_scatter(partial_value, "tp", scatter_dimension=0, tiled=True)


def kernel(Z, X, Y, C, tok, gain, up, down, out,
           tokg, upg, downg, hid, part, cin, zlo, zhi, zout, acc,
           wz_s, wz_r, wx_s, wx_r, wy_s, wy_r, wd_s, wd_r,
           tu_s, td_s, t_r, tc_s, tc_r, rc_s, rc_r, rz_s, rlo_r, rhi_r):
    T, D = tok.shape
    F = Z * X
    Dl = up.shape[0]
    B = upg.shape[2]
    fs, tp = lax.axis_index("fs"), lax.axis_index("tp")
    z, x = fs // X, fs % X
    y, c = tp // C, tp % C
    ox, oy, oc = X - 1 - x, Y - 1 - y, C - 1 - c

    def dev(zz=z, xx=x, yy=y, cc=c):
        return {"fs": zz * X + xx, "tp": yy * C + cc}

    def rcopy(src, dst, ss, rs, device):
        return pltpu.make_async_remote_copy(
            src_ref=src, dst_ref=dst, send_sem=ss, recv_sem=rs,
            device_id=device, device_id_type=MESH)

    barrier = pltpu.get_barrier_semaphore()
    peers = [dev(zz=(z + k) % Z) for k in range(1, Z)]
    peers += [dev(xx=ox), dev(yy=oy), dev(cc=oc)]
    for p in peers:
        pl.semaphore_signal(barrier, inc=1, device_id=p, device_id_type=MESH)

    def rows(cc):
        return pl.ds(pl.multiple_of(cc * T, T), T)

    mine = rows(c)

    pl.semaphore_wait(barrier, len(peers))

    def tok_up(g):
        return rcopy(tokg.at[g, mine], tokg.at[g, mine], tu_s.at[g], t_r.at[g], dev(zz=z + 1))

    def tok_dn(g):
        return rcopy(tokg.at[g, mine], tokg.at[g, mine], td_s.at[g], t_r.at[g], dev(zz=z - 1))

    def tok_c(g, cc=c):
        w = rows(cc)
        return rcopy(tokg.at[g, w], tokg.at[g, w], tc_s.at[g], tc_r.at[g], dev(cc=oc))

    def piece(zz, xx, yy, k):
        f = zz * X + xx
        if k == 0:
            return upg.at[yy, pl.ds(pl.multiple_of(f * Dl, Dl), Dl)]
        return downg.at[yy, f]

    def own_piece(zz, k):
        blk = pl.ds(pl.multiple_of(zz * B, B), B)
        return up.at[:, blk] if k == 0 else down.at[blk]

    def wz(zz, k):
        return rcopy(own_piece(zz, k), piece(z, x, y, k), wz_s.at[k, zz], wz_r.at[k, z], dev(zz=zz))

    def wz_recv(zz, k):
        p = piece(zz, x, y, k)
        return rcopy(p, p, wz_s.at[k, zz], wz_r.at[k, zz], dev(zz=zz))

    def wx(zz, k, xx=x):
        p = piece(zz, xx, y, k)
        return rcopy(p, p, wx_s.at[k, zz], wx_r.at[k, zz], dev(xx=ox))

    def wy(zz, k, yy=y):
        p = piece(zz, x, yy, k)
        return rcopy(p, p, wy_s.at[k, zz], wy_r.at[k, zz], dev(yy=oy))

    def wd(zz, k):
        if k == 0:
            p = piece(zz, ox, y, 0)
            return rcopy(p, p, wd_s.at[k, zz], wd_r.at[k, zz], dev(yy=oy))
        p = piece(zz, x, oy, 1)
        return rcopy(p, p, wd_s.at[k, zz], wd_r.at[k, zz], dev(xx=ox))

    def wd_recv(zz, k):
        p = piece(zz, ox, oy, k)
        return rcopy(p, p, wd_s.at[k, zz], wd_r.at[k, zz], dev(yy=oy) if k == 0 else dev(xx=ox))

    def each(d, body):
        for sgn in (-1, 1):
            zz = z + sgn * d

            @pl.when((zz >= 0) & (zz < Z))
            def _():
                body(zz, sgn)

    def tokens_out():
        @pl.when(z < Z - 1)
        def _():
            tok_up(z).start()

        @pl.when(z > 0)
        def _():
            tok_dn(z).start()

        tok_c(z).start()

    def weights_out(zz, sgn):
        wz(zz, 0).start()
        wz(zz, 1).start()

    def tokens_on(zz, sgn):
        tok_up(zz).wait_recv()
        if sgn < 0:
            @pl.when(z < Z - 1)
            def _():
                tok_up(zz).start()
        else:
            @pl.when(z > 0)
            def _():
                tok_dn(zz).start()
        tok_c(zz).start()

    def weights_on(zz, sgn):
        for k in range(2):
            wz_recv(zz, k).wait_recv()
            wx(zz, k).start()
            wy(zz, k).start()

    def diagonal(zz, sgn=0):
        wx(zz, 0, ox).wait_recv()
        wd(zz, 0).start()
        wy(zz, 1, oy).wait_recv()
        wd(zz, 1).start()

    def send_own_plane():
        for k in range(2):
            src, dst = own_piece(z, k), piece(z, x, y, k)
            rcopy(src, dst, wx_s.at[k, z], wx_r.at[k, z], dev(xx=ox)).start()
            rcopy(src, dst, wy_s.at[k, z], wy_r.at[k, z], dev(yy=oy)).start()

    def keep_own():
        own = pl.ds(pl.multiple_of(z * B, B), B)
        upg[y, pl.ds(pl.multiple_of(fs * Dl, Dl), Dl), :] = up[:, own]
        downg[y, fs] = down[own, :]

    for d in range(1, Z):
        each(d, weights_out)
    send_own_plane()
    RB = 32

    @pl.loop(0, T // RB)
    def _(i):
        r = pl.ds(pl.multiple_of(i * RB, RB), RB)
        v = tok[r, :].astype(f32)
        ms = jnp.mean(v * v, axis=-1, keepdims=True)
        w = pl.ds(pl.multiple_of(c * T + i * RB, RB), RB)
        tokg[z, w, :] = (v * lax.rsqrt(ms + epsilon) * gain[...]).astype(bf16)

    tokens_out()
    keep_own()
    diagonal(z)
    order = list(range(1, Z))
    for i, d in enumerate(order):
        each(d, weights_on)
        if i > 0:
            each(order[i - 1], diagonal)
            each(i, tokens_on)
    each(order[-1], diagonal)
    each(Z - 1, tokens_on)

    for g in range(Z):
        for k in range(2):
            wx(g, 1, ox).wait_recv() if k else wy(g, 0, oy).wait_recv()
            wd_recv(g, k).wait_recv()
        tok_c(g, oc).wait_recv()

    table = [sorted(range(Z), key=lambda g, a=a: -abs(g - a)) for a in range(Z)]

    def group(s):
        g = jnp.int32(table[0][s])
        for a in range(1, Z):
            g = jnp.where(z == a, jnp.int32(table[a][s]), g)
        return g

    NB = min(B, 256)

    def compute(g):
        for yy in range(Y):
            @pl.loop(0, B // NB)
            def _(j):
                cols = pl.ds(pl.multiple_of(j * NB, NB), NB)
                h = jnp.maximum(jnp.dot(tokg[g], upg[yy, :, cols], preferred_element_type=f32), 0.0)
                hid[yy, :, cols] = (h * h).astype(bf16)

    def project(g, h):
        @pl.loop(h * (F // H), (h + 1) * (F // H))
        def _(f):
            cols = pl.ds(pl.multiple_of(f * Dl, Dl), Dl)
            v = jnp.dot(hid[0], downg[0, f], preferred_element_type=f32)
            for yy in range(1, Y):
                v = v + jnp.dot(hid[yy], downg[yy, f], preferred_element_type=f32)
            v = v.astype(bf16)
            for cc in range(C):
                part[g, cc, :, cols] = v[cc * T:(cc + 1) * T]

    def cut(h):
        return pl.ds(h * (D // H), D // H)

    def sum_c(g, h):
        return rcopy(part.at[g, oc, :, cut(h)], cin.at[g, :, cut(h)], rc_s.at[h, g], rc_r.at[h, g], dev(cc=oc))

    def sum_up(g, h):
        return rcopy(zout.at[g, :, cut(h)], zlo.at[g, :, cut(h)], rz_s.at[h, g], rlo_r.at[h, g], dev(zz=z + 1))

    def sum_dn(g, h):
        return rcopy(zout.at[g, :, cut(h)], zhi.at[g, :, cut(h)], rz_s.at[h, g], rhi_r.at[h, g], dev(zz=z - 1))

    def step_z(g, h):
        w = cut(h)
        sum_c(g, h).wait_recv()
        acc[:, w] = part[g, c, :, w].astype(f32) + cin[g, :, w].astype(f32)

        @pl.when((z <= g) & (z > 0))
        def _():
            sum_up(g, h).wait_recv()
            acc[:, w] += zlo[g, :, w].astype(f32)

        @pl.when((z >= g) & (z < Z - 1))
        def _():
            sum_dn(g, h).wait_recv()
            acc[:, w] += zhi[g, :, w].astype(f32)

        @pl.when(z == g)
        def _():
            out[:, w] = acc[:, w].astype(bf16)

        @pl.when(z < g)
        def _():
            zout[g, :, w] = acc[:, w].astype(bf16)
            sum_up(g, h).start()

        @pl.when(z > g)
        def _():
            zout[g, :, w] = acc[:, w].astype(bf16)
            sum_dn(g, h).start()

    end = (z == 0) | (z == Z - 1)
    items = [(s, h) for s in range(Z) for h in range(H)]
    for i, (s, h) in enumerate(items):
        g = group(s)
        if h == 0:
            compute(g)
        project(g, h)
        sum_c(g, h).start()
        if i > 0 and items[i - 1][0] < Z - 1:
            @pl.when(end)
            def _():
                step_z(group(items[i - 1][0]), items[i - 1][1])
    for s, h in items:
        if s < Z - 1:
            @pl.when((z > 0) & (z < Z - 1))
            def _():
                step_z(group(s), h)
        else:
            step_z(group(s), h)

    for g in range(Z):
        @pl.when((z < Z - 1) & (g <= z))
        def _():
            tok_up(g).wait_send()

        @pl.when((z > 0) & (g >= z))
        def _():
            tok_dn(g).wait_send()

        tok_c(g).wait_send()
        for k in range(2):
            wx(g, k).wait_send()
            wy(g, k).wait_send()
            wd(g, k).wait_send()

        @pl.when(z != g)
        def _():
            wz(g, 0).wait_send()
            wz(g, 1).wait_send()
            for h in range(H):
                sum_up(g, h).wait_send()

        for h in range(H):
            sum_c(g, h).wait_send()


def solution(mesh):
    n_fs, n_tp = mesh.shape["fs"], mesh.shape["tp"]
    X = 2 ** (int(math.log2(n_fs)) // 2)
    Z = n_fs // X
    C = 2
    Y = n_tp // C
    placed = (P(("fs", "tp"), None), P(), P("fs", "tp"), P("tp", "fs"))

    def on_device(tokens, norm_gain, up_weight, down_weight):
        T, D = tokens.shape
        Dl, FFl = up_weight.shape
        B = FFl // Z
        if X != 2 or Y != 2 or Z * X != n_fs or Dl % 128 or B % 128 or T % 32 or D % (128 * H):
            return plain(tokens, norm_gain, up_weight, down_weight)
        F = Z * X
        dma = pltpu.SemaphoreType.DMA
        vm = pl.BlockSpec(memory_space=pltpu.VMEM)
        return pl.pallas_call(
            functools.partial(kernel, Z, X, Y, C),
            out_shape=jax.ShapeDtypeStruct((T, D), bf16),
            in_specs=[vm] * 4,
            out_specs=vm,
            scratch_shapes=[
                pltpu.VMEM((Z, C * T, D), bf16),
                pltpu.VMEM((Y, D, B), bf16),
                pltpu.VMEM((Y, F, B, Dl), bf16),
                pltpu.VMEM((Y, C * T, B), bf16),
                pltpu.VMEM((Z, C, T, D), bf16),
                pltpu.VMEM((Z, T, D), bf16),
                pltpu.VMEM((Z, T, D), bf16),
                pltpu.VMEM((Z, T, D), bf16),
                pltpu.VMEM((Z, T, D), bf16),
                pltpu.VMEM((T, D), f32),
                *[dma((2, Z)) for _ in range(8)],
                *[dma((Z,)) for _ in range(5)],
                *[dma((H, Z)) for _ in range(5)],
            ],
            compiler_params=pltpu.CompilerParams(
                collective_id=0, has_side_effects=True, vmem_limit_bytes=60 * 2**20),
        )(tokens, norm_gain.reshape(1, D), up_weight, down_weight)

    return jax.shard_map(
        on_device, mesh=mesh, in_specs=placed, out_specs=P(("fs", "tp"), None), check_vma=False)
```

profile of v0, /device:TPU:0, one launch (start us, length us, event | category | flops | bytes accessed | tf_op | source)
XLA Modules:
  0.0 130.1 jit_solution(7225959465469153157)
XLA Ops:
  0.0 128.2 %shard_map.46 = bf16[128,2048]{1,0:T(8,128)(2,1)} custom-call(bf16[128,2048]{1,0:T(8,128)(2,1)} %tok.1, f32[1,2048]{1,0:T(1,128)} %bitcast.1, bf16[256,2048]{1,0:T(8,128)(2,1)} %up.1, bf16[2048,256]{1,0:T(8,128)(2,1)} %down.1), custom_call_target="tpu_custom_call" | custom-call | tf_op jit(solution)/shard_map/pallas_call | solution.py:332
  128.2 1.9 %copy.6 = bf16[128,2048]{1,0:T(8,128)(2,1)} copy(bf16[128,2048]{1,0:T(8,128)(2,1)} %shard_map.46) | data formatting | bytes 1048576
where the time goes:
time: 130 us
  Pallas kernels  128 us (98%)
  local copies, waits for them, and re-layouts  1.88 us (1%)
    pallas_call x1, Pallas kernels, on_device(): pl.pallas_call(functools.partial(kernel, Z, X, Y, C), out_shape=jax.Shape...  128 us

commit v1 on v0

v1 whole, which is shorter than its diff:
```python
import functools
import math

import jax
import jax.numpy as jnp
from jax import lax
from jax.experimental import pallas as pl
from jax.experimental.pallas import tpu as pltpu
from jax.sharding import PartitionSpec as P

epsilon = 1e-06
MESH = pl.DeviceIdType.MESH
f32, bf16 = jnp.float32, jnp.bfloat16


def plain(tokens, norm_gain, up_weight, down_weight):
    values = tokens.astype(f32)
    mean_square = jnp.mean(values * values, axis=-1, keepdims=True)
    normed = (values * lax.rsqrt(mean_square + epsilon) * norm_gain).astype(bf16)
    up_whole = lax.all_gather(up_weight, "fs", axis=0, tiled=True)
    rows = lax.all_gather(normed, "tp", axis=0, tiled=True)
    preact = jnp.dot(rows, up_whole, preferred_element_type=f32)
    hidden = jnp.square(jnp.maximum(preact, 0.0)).astype(bf16)
    down_whole = lax.all_gather(down_weight, "fs", axis=1, tiled=True)
    partial_value = jnp.dot(hidden, down_whole, preferred_element_type=f32).astype(bf16)
    return lax.psum_scatter(partial_value, "tp", scatter_dimension=0, tiled=True)


PROGRAM = {
    0: [
        ("uown",), ("usend", 1), ("usend", 2), ("usend", 3), ("tsend",),
        ("urel", 1), ("udiag", 0), ("urel", 2), ("udiag", 1), ("urel", 3), ("udiag", 2),
        ("dsend", 1), ("udiag", 3), ("down_own",), ("trel", 1, 0), ("trel", 1, 1),
        ("trel", 2, 0), ("dsend", 2), ("dsend", 3), ("trel", 2, 1),
        ("uall", 0), ("uall", 1), ("uall", 2), ("uall", 3),
        ("hid", 0), ("hid", 1), ("drel", 1), ("ddiag", 0), ("hid", 2), ("ddiag", 1),
        ("trel", 3, 0), ("trel", 3, 1), ("dall", 0), ("hid", 3),
        ("proj", 0, (3, 2, 1, 0)), ("sum", 3, 0), ("sum", 2, 0), ("sum", 1, 0),
        ("dall", 1), ("proj", 1, (3, 2, 1, 0)), ("sum", 3, 1), ("sum", 2, 1), ("sum", 1, 1),
        ("drel", 2), ("ddiag", 2), ("drel", 3), ("ddiag", 3),
        ("dall", 2), ("proj", 2, (3, 2, 1, 0)), ("sum", 3, 2), ("sum", 2, 2), ("sum", 1, 2),
        ("dall", 3), ("proj", 3, (3, 2, 1, 0)), ("sum", 3, 3), ("sum", 2, 3), ("sum", 1, 3),
        ("sum", 0, 3), ("sum", 0, 2), ("sum", 0, 1), ("sum", 0, 0),
    ],
    1: [
        ("uown",), ("usend", 2), ("usend", 3), ("usend", 0), ("tsend",), ("dsend", 0),
        ("urel", 0), ("urel", 2), ("udiag", 1), ("udiag", 0), ("udiag", 2), ("urel", 3),
        ("udiag", 3), ("down_own",),
        ("trel", 0, 0), ("trel", 2, 0), ("trel", 0, 1), ("trel", 2, 1), ("dsend", 2), ("dsend", 3),
        ("uall", 0), ("uall", 1), ("uall", 2), ("uall", 3),
        ("hid", 1), ("ddiag", 1), ("hid", 0), ("trel", 3, 0), ("hid", 2), ("trel", 3, 1),
        ("drel", 0), ("ddiag", 0), ("hid", 3), ("dall", 1), ("proj", 1, (0, 1, 2, 3)),
        ("dall", 0), ("proj", 0, (3, 2, 1, 0)), ("sum", 3, 0), ("sum", 2, 0),
        ("drel", 3), ("ddiag", 3), ("drel", 2), ("ddiag", 2),
        ("dall", 3), ("proj", 3, (0, 1, 2, 3)), ("sum", 0, 3), ("sum", 3, 1), ("sum", 2, 1),
        ("dall", 2), ("proj", 2, (0, 1, 2, 3)), ("sum", 0, 2),
        ("sum", 3, 2), ("sum", 2, 2), ("sum", 0, 1), ("sum", 3, 3), ("sum", 2, 3), ("sum", 0, 0),
        ("sum", 1, 0), ("sum", 1, 1), ("sum", 1, 2), ("sum", 1, 3),
    ],
}


def kernel(Z, X, Y, C, tok, gain, up, down, out,
           tokb, upb, downb, tokg, upg, downg, hid, part, cin, zin, zout, outb,
           in_s, out_s, wz_s, wz_r, wx_s, wx_r, wy_s, wy_r, wd_s, wd_r,
           t_s, t_r, tc_s, tc_r, rc_s, rc_r, rz_s, rz_r):
    T, D = tok.shape
    F = Z * X
    Dl = up.shape[0]
    B = upg.shape[2]
    fs, tp = lax.axis_index("fs"), lax.axis_index("tp")
    z, x = fs // X, fs % X
    y, c = tp // C, tp % C
    ox, oy, oc = X - 1 - x, Y - 1 - y, C - 1 - c
    low = z < Z // 2
    p = jnp.where(low, z, Z - 1 - z)
    side = jnp.where(low, 0, 1)

    def plane(q):
        return jnp.where(low, q, Z - 1 - q)

    def dev(zz=z, xx=x, yy=y, cc=c):
        return {"fs": zz * X + xx, "tp": yy * C + cc}

    def rcopy(src, dst, ss, rs, device):
        return pltpu.make_async_remote_copy(
            src_ref=src, dst_ref=dst, send_sem=ss, recv_sem=rs,
            device_id=device, device_id_type=MESH)

    def rows(start, size):
        return pl.ds(pl.multiple_of(start, size), size)

    barrier = pltpu.get_barrier_semaphore()
    peers = [dev(zz=(z + k) % Z) for k in range(1, Z)]
    peers += [dev(xx=ox), dev(yy=oy), dev(cc=oc)]
    for peer in peers:
        pl.semaphore_signal(barrier, inc=1, device_id=peer, device_id_type=MESH)

    loads = [
        pltpu.make_async_copy(tok, tokb, in_s.at[0]),
        pltpu.make_async_copy(up, upb, in_s.at[1]),
        pltpu.make_async_copy(down, downb, in_s.at[2]),
        pltpu.make_async_copy(up.at[:, rows(z * B, B)], upg.at[y, rows(fs * Dl, Dl)], in_s.at[3]),
        pltpu.make_async_copy(down.at[rows(z * B, B)], downg.at[fs, rows(y * B, B)], in_s.at[4]),
    ]
    for load in loads:
        load.start()
    loads[0].wait()
    RB = 32

    @pl.loop(0, T // RB)
    def _(i):
        v = tokb[rows(i * RB, RB), :].astype(f32)
        ms = jnp.mean(v * v, axis=-1, keepdims=True)
        tokg[z, rows(c * T + i * RB, RB), :] = (v * lax.rsqrt(ms + epsilon) * gain[...]).astype(bf16)

    for load in loads[1:]:
        load.wait()
    pl.semaphore_wait(barrier, len(peers))

    def piece(zz, xx, yy, k, half=None):
        f = zz * X + xx
        if k == 0:
            r = rows(f * Dl, Dl) if half is None else rows(f * Dl + half * (Dl // 2), Dl // 2)
            return upg.at[yy, r]
        r = rows(yy * B, B) if half is None else rows(yy * B + half * (B // 2), B // 2)
        return downg.at[f, r]

    def own_piece(zz, k):
        return upb.at[:, rows(zz * B, B)] if k == 0 else downb.at[rows(zz * B, B)]

    def wz(q, k):
        zz = plane(q)
        return rcopy(own_piece(zz, k), piece(z, x, y, k), wz_s.at[k, zz], wz_r.at[k, z], dev(zz=zz))

    def wz_recv(q, k):
        zz = plane(q)
        ref = piece(zz, x, y, k)
        return rcopy(ref, ref, wz_s.at[k, zz], wz_r.at[k, zz], dev(zz=zz))

    def wx(q, k, xx=x):
        zz = plane(q)
        ref = piece(zz, xx, y, k)
        return rcopy(ref, ref, wx_s.at[k, zz], wx_r.at[k, zz], dev(xx=ox))

    def wy(q, k, yy=y):
        zz = plane(q)
        ref = piece(zz, x, yy, k)
        return rcopy(ref, ref, wy_s.at[k, zz], wy_r.at[k, zz], dev(yy=oy))

    def wd(q, k, half):
        zz = plane(q)
        ref = piece(zz, ox, y, k, 0) if half == 0 else piece(zz, x, oy, k, 1)
        to = dev(yy=oy) if half == 0 else dev(xx=ox)
        return rcopy(ref, ref, wd_s.at[k, zz, half], wd_r.at[k, zz, half], to)

    def wd_recv(q, k, half):
        zz = plane(q)
        ref = piece(zz, ox, oy, k, half)
        return rcopy(ref, ref, wd_s.at[k, zz, half], wd_r.at[k, zz, half], dev(yy=oy))

    TH = T // 2

    def tok_z(g, half, way):
        gg = plane(g)
        ref = tokg.at[gg, rows(c * T + half * TH, TH)]
        to = jnp.where(low, z + way, z - way)
        return rcopy(ref, ref, t_s.at[(way + 1) // 2, gg, half], t_r.at[gg, half], dev(zz=to))

    def tok_c(g, half, cc=c):
        gg = plane(g)
        ref = tokg.at[gg, rows(cc * T + half * TH, TH)]
        return rcopy(ref, ref, tc_s.at[gg, half], tc_r.at[gg, half], dev(cc=oc))

    NB = min(B, 256)

    def compute(g):
        gg = plane(g)
        for yy in range(Y):
            @pl.loop(0, B // NB)
            def _(j):
                h = jnp.dot(tokg[gg], upg[yy, :, rows(j * NB, NB)], preferred_element_type=f32)
                h = jnp.maximum(h, 0.0)
                hid[gg, :, rows(yy * B + j * NB, NB)] = (h * h).astype(bf16)

    def sum_c(gg, f):
        return rcopy(part.at[gg, f, oc], cin.at[gg, f], rc_s.at[gg, f], rc_r.at[gg, f], dev(cc=oc))

    def project(q, gs):
        for g in gs:
            gg = plane(g)

            @pl.loop(0, X)
            def _(xx):
                f = plane(q) * X + xx
                v = jnp.dot(hid[gg], downg[f], preferred_element_type=f32).astype(bf16)
                for cc in range(C):
                    part[gg, f, cc] = v[cc * T:(cc + 1) * T]
                sum_c(gg, f).start()

    def sum_z(gg, f, way):
        to = jnp.where(low, z + way, z - way)
        at = side if way > 0 else 1 - side
        return rcopy(zout.at[gg, f], zin.at[at, gg, f], rz_s.at[gg, f], rz_r.at[at, gg, f], dev(zz=to))

    def out_copy(f):
        cols = rows(f * Dl, Dl)
        return pltpu.make_async_copy(outb.at[:, cols], out.at[:, cols], out_s.at[f])

    def step(me, g, q):
        gg = plane(g)

        @pl.loop(0, X)
        def _(xx):
            f = plane(q) * X + xx
            sum_c(gg, f).wait_recv()
            acc = part[gg, f, c].astype(f32) + cin[gg, f].astype(f32)
            if me > 0 and g >= me:
                sum_z(gg, f, 1).wait_recv()
                acc = acc + zin[side, gg, f].astype(f32)
            if g <= me:
                sum_z(gg, f, -1).wait_recv()
                acc = acc + zin[1 - side, gg, f].astype(f32)
            if g == me:
                outb[:, rows(f * Dl, Dl)] = acc.astype(bf16)
                out_copy(f).start()
            else:
                zout[gg, f] = acc.astype(bf16)
                sum_z(gg, f, 1 if g > me else -1).start()

    def run(me, op, *args):
        if op == "uown" or op == "down_own":
            k = 0 if op == "uown" else 1
            wx(me, k).start()
            wy(me, k).start()
        elif op == "usend" or op == "dsend":
            wz(args[0], 0 if op == "usend" else 1).start()
        elif op == "urel" or op == "drel":
            k = 0 if op == "urel" else 1
            wz_recv(args[0], k).wait_recv()
            wx(args[0], k).start()
            wy(args[0], k).start()
        elif op == "udiag" or op == "ddiag":
            k = 0 if op == "udiag" else 1
            wx(args[0], k, ox).wait_recv()
            wd(args[0], k, 0).start()
            wy(args[0], k, oy).wait_recv()
            wd(args[0], k, 1).start()
        elif op == "uall" or op == "dall":
            k = 0 if op == "uall" else 1
            for half in range(2):
                wd_recv(args[0], k, half).wait_recv()
        elif op == "tsend":
            for half in range(2):
                tok_z(me, half, 1).start()
                if me > 0:
                    tok_z(me, half, -1).start()
            for half in range(2):
                tok_c(me, half).start()
        elif op == "trel":
            g, half = args
            tok_z(g, half, 1 if g < me else -1).wait_recv()
            if me > 0:
                tok_z(g, half, 1 if g < me else -1).start()
            tok_c(g, half).start()
        elif op == "hid":
            for half in range(2):
                tok_c(args[0], half, oc).wait_recv()
            compute(args[0])
        elif op == "proj":
            project(*args)
        elif op == "sum":
            step(me, *args)

    def drain(me):
        for q in range(Z):
            for k in range(2):
                if q != me:
                    wz(q, k).wait_send()
                wx(q, k).wait_send()
                wy(q, k).wait_send()
                for half in range(2):
                    wd(q, k, half).wait_send()
            for half in range(2):
                tok_c(q, half).wait_send()
                if q == me or me > 0:
                    if q <= me:
                        tok_z(q, half, 1).wait_send()
                    if q >= me and me > 0:
                        tok_z(q, half, -1).wait_send()

    for me in range(Z // 2):
        @pl.when(p == me)
        def _(me=me):
            for item in PROGRAM[me]:
                run(me, *item)
            drain(me)

    @pl.loop(0, F)
    def _(f):
        @pl.loop(0, Z)
        def _(gg):
            sum_c(gg, f).wait_send()

            @pl.when(gg != z)
            def _():
                sum_z(gg, f, 1).wait_send()
        out_copy(f).wait()


def solution(mesh):
    n_fs, n_tp = mesh.shape["fs"], mesh.shape["tp"]
    X = 2 ** (int(math.log2(n_fs)) // 2)
    Z = n_fs // X
    C = 2
    Y = n_tp // C
    placed = (P(("fs", "tp"), None), P(), P("fs", "tp"), P("tp", "fs"))

    def on_device(tokens, norm_gain, up_weight, down_weight):
        T, D = tokens.shape
        Dl, FFl = up_weight.shape
        B = FFl // Z
        if X != 2 or Y != 2 or Z != 4 or Z * X != n_fs or Dl % 256 or B % 256 or T % 32:
            return plain(tokens, norm_gain, up_weight, down_weight)
        F = Z * X
        dma = pltpu.SemaphoreType.DMA
        vm = pl.BlockSpec(memory_space=pltpu.VMEM)
        hbm = pl.BlockSpec(memory_space=pl.ANY)
        return pl.pallas_call(
            functools.partial(kernel, Z, X, Y, C),
            out_shape=jax.ShapeDtypeStruct((T, D), bf16),
            in_specs=[hbm, vm, hbm, hbm],
            out_specs=hbm,
            scratch_shapes=[
                pltpu.VMEM((T, D), bf16),
                pltpu.VMEM((Dl, FFl), bf16),
                pltpu.VMEM((FFl, Dl), bf16),
                pltpu.VMEM((Z, C * T, D), bf16),
                pltpu.VMEM((Y, D, B), bf16),
                pltpu.VMEM((F, Y * B, Dl), bf16),
                pltpu.VMEM((Z, C * T, Y * B), bf16),
                pltpu.VMEM((Z, F, C, T, Dl), bf16),
                pltpu.VMEM((Z, F, T, Dl), bf16),
                pltpu.VMEM((2, Z, F, T, Dl), bf16),
                pltpu.VMEM((Z, F, T, Dl), bf16),
                pltpu.VMEM((T, D), bf16),
                dma((5,)), dma((F,)),
                *[dma((2, Z)) for _ in range(6)],
                *[dma((2, Z, 2)) for _ in range(2)],
                dma((2, Z, 2)), dma((Z, 2)), dma((Z, 2)), dma((Z, 2)),
                dma((Z, F)), dma((Z, F)), dma((Z, F)), dma((2, Z, F)),
            ],
            compiler_params=pltpu.CompilerParams(
                collective_id=0, has_side_effects=True, vmem_limit_bytes=60 * 2**20),
        )(tokens, norm_gain.reshape(1, D), up_weight, down_weight)

    return jax.shard_map(
        on_device, mesh=mesh, in_specs=placed, out_specs=P(("fs", "tp"), None), check_vma=False)
```

time: 130 us -> 135 us (1.038)
  Pallas kernels: 128 us -> 133 us
    pallas_call x1, Pallas kernels: 128 us -> 133 us  [on_device(): pl.pallas_call(functools.partial(kernel, Z, X, Y, C), out_shape=jax.Shape...]
where the time goes in v1:
time: 135 us
  Pallas kernels  133 us (99%)
  local copies, waits for them, and re-layouts  1.88 us (1%)
    pallas_call x1, Pallas kernels, on_device(): pl.pallas_call(functools.partial(kernel, Z, X, Y, C), out_shape=jax.Shape...  133 us

profile of v1, /device:TPU:0, one launch (start us, length us, event | category | flops | bytes accessed | tf_op | source)
XLA Modules:
  0.0 134.6 jit_solution(1192886182826716716)
XLA Ops:
  0.0 132.7 %shard_map.46 = bf16[128,2048]{1,0:T(8,128)(2,1)} custom-call(bf16[128,2048]{1,0:T(8,128)(2,1)} %tok.1, f32[1,2048]{1,0:T(1,128)} %bitcast.1, bf16[256,2048]{1,0:T(8,128)(2,1)} %up.1, bf16[2048,256]{1,0:T(8,128)(2,1)} %down.1), custom_call_target="tpu_custom_call" | custom-call | tf_op jit(solution)/shard_map/pallas_call | solution.py:329
  132.7 1.9 %copy.6 = bf16[128,2048]{1,0:T(8,128)(2,1)} copy(bf16[128,2048]{1,0:T(8,128)(2,1)} %shard_map.46) | data formatting | bytes 1048576

commit v2 on v1

--- a/solution.py
+++ b/solution.py
@@ -28,34 +28,32 @@
 
 PROGRAM = {
     0: [
-        ("uown",), ("usend", 1), ("usend", 2), ("usend", 3), ("tsend",),
-        ("urel", 1), ("udiag", 0), ("urel", 2), ("udiag", 1), ("urel", 3), ("udiag", 2),
-        ("dsend", 1), ("udiag", 3), ("down_own",), ("trel", 1, 0), ("trel", 1, 1),
-        ("trel", 2, 0), ("dsend", 2), ("dsend", 3), ("trel", 2, 1),
-        ("uall", 0), ("uall", 1), ("uall", 2), ("uall", 3),
-        ("hid", 0), ("hid", 1), ("drel", 1), ("ddiag", 0), ("hid", 2), ("ddiag", 1),
-        ("trel", 3, 0), ("trel", 3, 1), ("dall", 0), ("hid", 3),
-        ("proj", 0, (3, 2, 1, 0)), ("sum", 3, 0), ("sum", 2, 0), ("sum", 1, 0),
-        ("dall", 1), ("proj", 1, (3, 2, 1, 0)), ("sum", 3, 1), ("sum", 2, 1), ("sum", 1, 1),
-        ("drel", 2), ("ddiag", 2), ("drel", 3), ("ddiag", 3),
-        ("dall", 2), ("proj", 2, (3, 2, 1, 0)), ("sum", 3, 2), ("sum", 2, 2), ("sum", 1, 2),
-        ("dall", 3), ("proj", 3, (3, 2, 1, 0)), ("sum", 3, 3), ("sum", 2, 3), ("sum", 1, 3),
-        ("sum", 0, 3), ("sum", 0, 2), ("sum", 0, 1), ("sum", 0, 0),
+        ("uown",), ("usend", 3), ("usend", 2), ("usend", 1), ("tsend",), ("dsend", 1),
+        ("udiag", 0), ("urel", 3), ("urel", 1), ("udiag", 3), ("udiag", 1), ("urel", 2), ("udiag", 2),
+        ("down_own",), ("drel", 1), ("trel", 1, 0), ("trel", 1, 1),
+        ("uall", 0), ("uall", 1), ("uall", 2), ("uall", 3), ("hid", 0), ("hid", 1),
+        ("dsend", 3), ("dsend", 2), ("ddiag", 0), ("trel", 2, 0), ("dall", 0),
+        ("proj", 0, (1, 0)), ("sum", 1, 0), ("ddiag", 1), ("trel", 2, 1), ("drel", 3), ("hid", 2),
+        ("proj", 0, (2,)), ("sum", 2, 0), ("dall", 1), ("proj", 1, (2, 1, 0)), ("sum", 2, 1), ("sum", 1, 1),
+        ("trel", 3, 0), ("ddiag", 3), ("dall", 3), ("proj", 3, (2, 1, 0)), ("sum", 2, 3), ("sum", 1, 3),
+        ("trel", 3, 1), ("drel", 2), ("hid", 3),
+        ("proj", 0, (3,)), ("sum", 3, 0), ("proj", 1, (3,)), ("sum", 3, 1), ("proj", 3, (3,)), ("sum", 3, 3),
+        ("ddiag", 2), ("dall", 2), ("proj", 2, (3, 2, 1, 0)), ("sum", 3, 2), ("sum", 2, 2), ("sum", 1, 2),
+        ("sum", 0, 3), ("sum", 0, 2), ("sum", 0, 0), ("sum", 0, 1),
     ],
     1: [
         ("uown",), ("usend", 2), ("usend", 3), ("usend", 0), ("tsend",), ("dsend", 0),
-        ("urel", 0), ("urel", 2), ("udiag", 1), ("udiag", 0), ("udiag", 2), ("urel", 3),
-        ("udiag", 3), ("down_own",),
-        ("trel", 0, 0), ("trel", 2, 0), ("trel", 0, 1), ("trel", 2, 1), ("dsend", 2), ("dsend", 3),
+        ("udiag", 1), ("urel", 3), ("urel", 0), ("urel", 2), ("udiag", 3), ("trel", 0, 0), ("udiag", 0),
+        ("trel", 0, 1), ("trel", 2, 0), ("udiag", 2), ("down_own",), ("trel", 2, 1),
+        ("dsend", 2), ("dsend", 3), ("drel", 0),
         ("uall", 0), ("uall", 1), ("uall", 2), ("uall", 3),
-        ("hid", 1), ("ddiag", 1), ("hid", 0), ("trel", 3, 0), ("hid", 2), ("trel", 3, 1),
-        ("drel", 0), ("ddiag", 0), ("hid", 3), ("dall", 1), ("proj", 1, (0, 1, 2, 3)),
-        ("dall", 0), ("proj", 0, (3, 2, 1, 0)), ("sum", 3, 0), ("sum", 2, 0),
-        ("drel", 3), ("ddiag", 3), ("drel", 2), ("ddiag", 2),
-        ("dall", 3), ("proj", 3, (0, 1, 2, 3)), ("sum", 0, 3), ("sum", 3, 1), ("sum", 2, 1),
-        ("dall", 2), ("proj", 2, (0, 1, 2, 3)), ("sum", 0, 2),
-        ("sum", 3, 2), ("sum", 2, 2), ("sum", 0, 1), ("sum", 3, 3), ("sum", 2, 3), ("sum", 0, 0),
-        ("sum", 1, 0), ("sum", 1, 1), ("sum", 1, 2), ("sum", 1, 3),
+        ("hid", 1), ("hid", 0), ("trel", 3, 0), ("ddiag", 1), ("hid", 2), ("dall", 1), ("proj", 1, (2, 0, 1)),
+        ("ddiag", 0), ("drel", 3), ("dall", 0), ("trel", 3, 1), ("proj", 0, (2, 0, 1)), ("sum", 2, 0),
+        ("drel", 2), ("hid", 3), ("proj", 1, (3,)), ("proj", 0, (3,)), ("sum", 2, 1), ("ddiag", 3),
+        ("dall", 3), ("proj", 3, (2, 3, 0, 1)), ("sum", 2, 3), ("ddiag", 2), ("sum", 3, 0), ("sum", 0, 3),
+        ("sum", 3, 1), ("sum", 3, 3), ("sum", 0, 0),
+        ("dall", 2), ("proj", 2, (0, 3, 2, 1)), ("sum", 0, 2), ("sum", 3, 2), ("sum", 2, 2), ("sum", 0, 1),
+        ("sum", 1, 0), ("sum", 1, 3), ("sum", 1, 1), ("sum", 1, 2),
     ],
 }
 

time: 135 us -> 113 us (0.84)
  Pallas kernels: 133 us -> 111 us
    pallas_call x1, Pallas kernels: 133 us -> 111 us  [on_device(): pl.pallas_call(functools.partial(kernel, Z, X, Y, C), out_shape=jax.Shape...]
where the time goes in v2:
time: 113 us
  Pallas kernels  111 us (98%)
  local copies, waits for them, and re-layouts  1.88 us (2%)
    pallas_call x1, Pallas kernels, on_device(): pl.pallas_call(functools.partial(kernel, Z, X, Y, C), out_shape=jax.Shape...  111 us

profile of v2, /device:TPU:0, one launch (start us, length us, event | category | flops | bytes accessed | tf_op | source)
XLA Modules:
  0.0 112.6 jit_solution(1365704298482611904)
XLA Ops:
  0.0 110.7 %shard_map.46 = bf16[128,2048]{1,0:T(8,128)(2,1)} custom-call(bf16[128,2048]{1,0:T(8,128)(2,1)} %tok.1, f32[1,2048]{1,0:T(1,128)} %bitcast.1, bf16[256,2048]{1,0:T(8,128)(2,1)} %up.1, bf16[2048,256]{1,0:T(8,128)(2,1)} %down.1), custom_call_target="tpu_custom_call" | custom-call | tf_op jit(solution)/shard_map/pallas_call | solution.py:327
  110.7 1.9 %copy.6 = bf16[128,2048]{1,0:T(8,128)(2,1)} copy(bf16[128,2048]{1,0:T(8,128)(2,1)} %shard_map.46) | data formatting | bytes 1048576

commit v3 on v2

--- a/solution.py
+++ b/solution.py
@@ -29,30 +29,38 @@
 PROGRAM = {
     0: [
         ("uown",), ("usend", 3), ("usend", 2), ("usend", 1), ("tsend",), ("dsend", 1),
-        ("udiag", 0), ("urel", 3), ("urel", 1), ("udiag", 3), ("udiag", 1), ("urel", 2), ("udiag", 2),
-        ("down_own",), ("drel", 1), ("trel", 1, 0), ("trel", 1, 1),
-        ("uall", 0), ("uall", 1), ("uall", 2), ("uall", 3), ("hid", 0), ("hid", 1),
-        ("dsend", 3), ("dsend", 2), ("ddiag", 0), ("trel", 2, 0), ("dall", 0),
-        ("proj", 0, (1, 0)), ("sum", 1, 0), ("ddiag", 1), ("trel", 2, 1), ("drel", 3), ("hid", 2),
-        ("proj", 0, (2,)), ("sum", 2, 0), ("dall", 1), ("proj", 1, (2, 1, 0)), ("sum", 2, 1), ("sum", 1, 1),
-        ("trel", 3, 0), ("ddiag", 3), ("dall", 3), ("proj", 3, (2, 1, 0)), ("sum", 2, 3), ("sum", 1, 3),
-        ("trel", 3, 1), ("drel", 2), ("hid", 3),
-        ("proj", 0, (3,)), ("sum", 3, 0), ("proj", 1, (3,)), ("sum", 3, 1), ("proj", 3, (3,)), ("sum", 3, 3),
-        ("ddiag", 2), ("dall", 2), ("proj", 2, (3, 2, 1, 0)), ("sum", 3, 2), ("sum", 2, 2), ("sum", 1, 2),
+        ("udiag", 0, 0), ("urel", 3, 0), ("udiag", 0, 1), ("urel", 3, 1), ("urel", 1, 0), ("udiag", 3, 0),
+        ("urel", 1, 1), ("udiag", 3, 1), ("udiag", 1, 0), ("urel", 2, 0), ("udiag", 1, 1), ("urel", 2, 1),
+        ("udiag", 2, 0), ("udiag", 2, 1),
+        ("down_own",), ("drel", 1, 0), ("drel", 1, 1), ("trel", 1, 0), ("trel", 1, 1),
+        ("uall", 0), ("uall", 1), ("uall", 3), ("uall", 2), ("hid", 0), ("hid", 1),
+        ("dsend", 3), ("dsend", 2), ("ddiag", 0, 0), ("trel", 2, 0), ("ddiag", 0, 1),
+        ("ddiag", 1, 0), ("dall", 0),
+        ("proj", 0, (1, 0)), ("ddiag", 1, 1), ("sum", 1, 0), ("trel", 2, 1), ("drel", 3, 0), ("drel", 3, 1), ("hid", 2),
+        ("proj", 0, (2,)), ("dall", 1), ("proj", 1, (2, 1, 0)), ("sum", 2, 0), ("sum", 2, 1), ("sum", 1, 1),
+        ("trel", 3, 0), ("ddiag", 3, 0), ("ddiag", 3, 1), ("dall", 3),
+        ("proj", 3, (2, 1, 0)), ("sum", 2, 3), ("sum", 1, 3),
+        ("trel", 3, 1), ("drel", 2, 0), ("hid", 3), ("drel", 2, 1),
+        ("proj", 0, (3,)), ("proj", 1, (3,)), ("sum", 3, 0), ("ddiag", 2, 0), ("proj", 3, (3,)), ("sum", 3, 1),
+        ("sum", 3, 3), ("ddiag", 2, 1), ("dall", 2),
+        ("proj", 2, (3,)), ("proj", 2, (2,)), ("sum", 3, 2), ("proj", 2, (1,)), ("sum", 2, 2),
+        ("proj", 2, (0,)), ("sum", 1, 2),
         ("sum", 0, 3), ("sum", 0, 2), ("sum", 0, 0), ("sum", 0, 1),
     ],
     1: [
         ("uown",), ("usend", 2), ("usend", 3), ("usend", 0), ("tsend",), ("dsend", 0),
-        ("udiag", 1), ("urel", 3), ("urel", 0), ("urel", 2), ("udiag", 3), ("trel", 0, 0), ("udiag", 0),
-        ("trel", 0, 1), ("trel", 2, 0), ("udiag", 2), ("down_own",), ("trel", 2, 1),
-        ("dsend", 2), ("dsend", 3), ("drel", 0),
-        ("uall", 0), ("uall", 1), ("uall", 2), ("uall", 3),
-        ("hid", 1), ("hid", 0), ("trel", 3, 0), ("ddiag", 1), ("hid", 2), ("dall", 1), ("proj", 1, (2, 0, 1)),
-        ("ddiag", 0), ("drel", 3), ("dall", 0), ("trel", 3, 1), ("proj", 0, (2, 0, 1)), ("sum", 2, 0),
-        ("drel", 2), ("hid", 3), ("proj", 1, (3,)), ("proj", 0, (3,)), ("sum", 2, 1), ("ddiag", 3),
-        ("dall", 3), ("proj", 3, (2, 3, 0, 1)), ("sum", 2, 3), ("ddiag", 2), ("sum", 3, 0), ("sum", 0, 3),
-        ("sum", 3, 1), ("sum", 3, 3), ("sum", 0, 0),
-        ("dall", 2), ("proj", 2, (0, 3, 2, 1)), ("sum", 0, 2), ("sum", 3, 2), ("sum", 2, 2), ("sum", 0, 1),
+        ("udiag", 1, 0), ("udiag", 1, 1), ("urel", 3, 0), ("urel", 3, 1), ("udiag", 3, 0),
+        ("urel", 0, 0), ("urel", 2, 0), ("udiag", 3, 1), ("urel", 0, 1), ("urel", 2, 1),
+        ("udiag", 0, 0), ("udiag", 2, 0), ("trel", 0, 0), ("udiag", 0, 1), ("trel", 2, 0), ("trel", 0, 1),
+        ("udiag", 2, 1), ("down_own",), ("trel", 2, 1), ("dsend", 2), ("dsend", 3), ("drel", 0, 0), ("drel", 0, 1),
+        ("uall", 1), ("uall", 3), ("uall", 0), ("uall", 2),
+        ("hid", 1), ("hid", 0), ("ddiag", 1, 0), ("trel", 3, 0), ("ddiag", 1, 1), ("hid", 2),
+        ("ddiag", 0, 0), ("dall", 1), ("proj", 1, (2, 0, 1)), ("ddiag", 0, 1), ("drel", 3, 0), ("drel", 3, 1),
+        ("trel", 3, 1), ("dall", 0), ("proj", 0, (2, 0, 1)), ("sum", 2, 0), ("drel", 2, 0), ("drel", 2, 1),
+        ("hid", 3), ("ddiag", 3, 0), ("proj", 1, (3,)), ("proj", 0, (3,)), ("ddiag", 3, 1), ("sum", 2, 1),
+        ("dall", 3), ("proj", 3, (2, 3, 0, 1)), ("sum", 2, 3), ("ddiag", 2, 0), ("ddiag", 2, 1),
+        ("sum", 3, 0), ("sum", 3, 1), ("dall", 2), ("proj", 2, (0, 3, 2, 1)), ("sum", 0, 3), ("sum", 3, 3),
+        ("sum", 0, 2), ("sum", 0, 0), ("sum", 3, 2), ("sum", 2, 2), ("sum", 0, 1),
         ("sum", 1, 0), ("sum", 1, 3), ("sum", 1, 1), ("sum", 1, 2),
     ],
 }
@@ -116,35 +124,36 @@
         load.wait()
     pl.semaphore_wait(barrier, len(peers))
 
-    def piece(zz, xx, yy, k, half=None):
+    def piece(zz, xx, yy, k, half):
         f = zz * X + xx
         if k == 0:
-            r = rows(f * Dl, Dl) if half is None else rows(f * Dl + half * (Dl // 2), Dl // 2)
-            return upg.at[yy, r]
-        r = rows(yy * B, B) if half is None else rows(yy * B + half * (B // 2), B // 2)
-        return downg.at[f, r]
-
-    def own_piece(zz, k):
-        return upb.at[:, rows(zz * B, B)] if k == 0 else downb.at[rows(zz * B, B)]
-
-    def wz(q, k):
-        zz = plane(q)
-        return rcopy(own_piece(zz, k), piece(z, x, y, k), wz_s.at[k, zz], wz_r.at[k, z], dev(zz=zz))
-
-    def wz_recv(q, k):
-        zz = plane(q)
-        ref = piece(zz, x, y, k)
-        return rcopy(ref, ref, wz_s.at[k, zz], wz_r.at[k, zz], dev(zz=zz))
-
-    def wx(q, k, xx=x):
-        zz = plane(q)
-        ref = piece(zz, xx, y, k)
-        return rcopy(ref, ref, wx_s.at[k, zz], wx_r.at[k, zz], dev(xx=ox))
-
-    def wy(q, k, yy=y):
-        zz = plane(q)
-        ref = piece(zz, x, yy, k)
-        return rcopy(ref, ref, wy_s.at[k, zz], wy_r.at[k, zz], dev(yy=oy))
+            return upg.at[yy, rows(f * Dl + half * (Dl // 2), Dl // 2)]
+        return downg.at[f, rows(yy * B + half * (B // 2), B // 2)]
+
+    def own_piece(zz, k, half):
+        if k == 0:
+            return upb.at[rows(half * (Dl // 2), Dl // 2), rows(zz * B, B)]
+        return downb.at[rows(zz * B + half * (B // 2), B // 2)]
+
+    def wz(q, k, half):
+        zz = plane(q)
+        return rcopy(own_piece(zz, k, half), piece(z, x, y, k, half),
+                     wz_s.at[k, zz, half], wz_r.at[k, z, half], dev(zz=zz))
+
+    def wz_recv(q, k, half):
+        zz = plane(q)
+        ref = piece(zz, x, y, k, half)
+        return rcopy(ref, ref, wz_s.at[k, zz, half], wz_r.at[k, zz, half], dev(zz=zz))
+
+    def wx(q, k, half, xx=x):
+        zz = plane(q)
+        ref = piece(zz, xx, y, k, half)
+        return rcopy(ref, ref, wx_s.at[k, zz, half], wx_r.at[k, zz, half], dev(xx=ox))
+
+    def wy(q, k, half, yy=y):
+        zz = plane(q)
+        ref = piece(zz, x, yy, k, half)
+        return rcopy(ref, ref, wy_s.at[k, zz, half], wy_r.at[k, zz, half], dev(yy=oy))
 
     def wd(q, k, half):
         zz = plane(q)
@@ -227,27 +236,32 @@
                 sum_z(gg, f, 1 if g > me else -1).start()
 
     def run(me, op, *args):
+        k = 0 if op[0] == "u" else 1
         if op == "uown" or op == "down_own":
-            k = 0 if op == "uown" else 1
-            wx(me, k).start()
-            wy(me, k).start()
+            for half in range(2):
+                wx(me, k, half).start()
+                wy(me, k, half).start()
         elif op == "usend" or op == "dsend":
-            wz(args[0], 0 if op == "usend" else 1).start()
+            for half in range(2):
+                wz(args[0], k, half).start()
         elif op == "urel" or op == "drel":
-            k = 0 if op == "urel" else 1
-            wz_recv(args[0], k).wait_recv()
-            wx(args[0], k).start()
-            wy(args[0], k).start()
+            q, half = args
+            wz_recv(q, k, half).wait_recv()
+            wx(q, k, half).start()
+            wy(q, k, half).start()
         elif op == "udiag" or op == "ddiag":
-            k = 0 if op == "udiag" else 1
-            wx(args[0], k, ox).wait_recv()
-            wd(args[0], k, 0).start()
-            wy(args[0], k, oy).wait_recv()
-            wd(args[0], k, 1).start()
+            q, half = args
+            if half == 0:
+                wx(q, k, 0, ox).wait_recv()
+            else:
+                wy(q, k, 1, oy).wait_recv()
+            wd(q, k, half).start()
         elif op == "uall" or op == "dall":
-            k = 0 if op == "uall" else 1
-            for half in range(2):
-                wd_recv(args[0], k, half).wait_recv()
+            q = args[0]
+            wx(q, k, 1, ox).wait_recv()
+            wy(q, k, 0, oy).wait_recv()
+            for half in range(2):
+                wd_recv(q, k, half).wait_recv()
         elif op == "tsend":
             for half in range(2):
                 tok_z(me, half, 1).start()
@@ -273,11 +287,11 @@
     def drain(me):
         for q in range(Z):
             for k in range(2):
-                if q != me:
-                    wz(q, k).wait_send()
-                wx(q, k).wait_send()
-                wy(q, k).wait_send()
                 for half in range(2):
+                    if q != me:
+                        wz(q, k, half).wait_send()
+                    wx(q, k, half).wait_send()
+                    wy(q, k, half).wait_send()
                     wd(q, k, half).wait_send()
             for half in range(2):
                 tok_c(q, half).wait_send()
@@ -343,8 +357,7 @@
                 pltpu.VMEM((Z, F, T, Dl), bf16),
                 pltpu.VMEM((T, D), bf16),
                 dma((5,)), dma((F,)),
-                *[dma((2, Z)) for _ in range(6)],
-                *[dma((2, Z, 2)) for _ in range(2)],
+                *[dma((2, Z, 2)) for _ in range(8)],
                 dma((2, Z, 2)), dma((Z, 2)), dma((Z, 2)), dma((Z, 2)),
                 dma((Z, F)), dma((Z, F)), dma((Z, F)), dma((2, Z, F)),
             ],

time: 113 us -> 109 us (0.965)
  Pallas kernels: 111 us -> 107 us
    pallas_call x1, Pallas kernels: 111 us -> 107 us  [on_device(): pl.pallas_call(functools.partial(kernel, Z, X, Y, C), out_shape=jax.Shape...]
where the time goes in v3:
time: 109 us; the launch traced here: 108 us
  Pallas kernels  107 us (98%)
  local copies, waits for them, and re-layouts  1.88 us (2%)
    pallas_call x1, Pallas kernels, on_device(): pl.pallas_call(functools.partial(kernel, Z, X, Y, C), out_shape=jax.Shape...  107 us

profile of v3, /device:TPU:0, one launch (start us, length us, event | category | flops | bytes accessed | tf_op | source)
XLA Modules:
  0.0 108.4 jit_solution(14565765212024673957)
XLA Ops:
  0.0 106.5 %shard_map.46 = bf16[128,2048]{1,0:T(8,128)(2,1)} custom-call(bf16[128,2048]{1,0:T(8,128)(2,1)} %tok.1, f32[1,2048]{1,0:T(1,128)} %bitcast.1, bf16[256,2048]{1,0:T(8,128)(2,1)} %up.1, bf16[2048,256]{1,0:T(8,128)(2,1)} %down.1), custom_call_target="tpu_custom_call" | custom-call | tf_op jit(solution)/shard_map/pallas_call | solution.py:341
  106.5 1.9 %copy.6 = bf16[128,2048]{1,0:T(8,128)(2,1)} copy(bf16[128,2048]{1,0:T(8,128)(2,1)} %shard_map.46) | data formatting | bytes 1048576

commit v4 on v3

v4 whole, which is shorter than its diff:
```python
import functools
import math

import jax
import jax.numpy as jnp
from jax import lax
from jax.experimental import pallas as pl
from jax.experimental.pallas import tpu as pltpu
from jax.sharding import PartitionSpec as P

epsilon = 1e-06
MESH = pl.DeviceIdType.MESH
CUTS = 4
f32, bf16 = jnp.float32, jnp.bfloat16


def plain(tokens, norm_gain, up_weight, down_weight):
    values = tokens.astype(f32)
    mean_square = jnp.mean(values * values, axis=-1, keepdims=True)
    normed = (values * lax.rsqrt(mean_square + epsilon) * norm_gain).astype(bf16)
    up_whole = lax.all_gather(up_weight, "fs", axis=0, tiled=True)
    rows = lax.all_gather(normed, "tp", axis=0, tiled=True)
    preact = jnp.dot(rows, up_whole, preferred_element_type=f32)
    hidden = jnp.square(jnp.maximum(preact, 0.0)).astype(bf16)
    down_whole = lax.all_gather(down_weight, "fs", axis=1, tiled=True)
    partial_value = jnp.dot(hidden, down_whole, preferred_element_type=f32).astype(bf16)
    return lax.psum_scatter(partial_value, "tp", scatter_dimension=0, tiled=True)


PROGRAM = {
    0: [
        ("uown",), ("usend", 3, 1), ("usend", 1, 1), ("norm",), ("down_own",), ("tsend", 0, 1), ("tsend", 2, 1),
        ("urel", 3, 1), ("dsend", 3, 1), ("urel", 2, 1), ("usend", 1, 0), ("ddiag", 0, 1), ("ddiag", 0, 0),
        ("dsend", 1, 0), ("dsend", 3, 0), ("usend", 2, 0), ("dsend", 2, 1), ("udiag", 0, 0), ("tsend", 1, 0),
        ("urel", 2, 0), ("drel", 3, 1), ("usend", 3, 0), ("urel", 1, 0), ("udiag", 3, 1), ("drel", 3, 0),
        ("urel", 1, 1), ("usend", 2, 1), ("udiag", 2, 0), ("tsend", 3, 1), ("urel", 3, 0), ("trel", 1, 1),
        ("tsend", 1, 1), ("udiag", 0, 1), ("ddiag", 3, 0), ("udiag", 2, 1), ("tsend", 3, 0), ("udiag", 1, 0),
        ("dall", 0), ("udiag", 3, 0), ("ddiag", 3, 1), ("udiag", 1, 1), ("trel", 1, 2), ("trel", 2, 0),
        ("dsend", 1, 1), ("tsend", 0, 0), ("trel", 1, 3), ("trel", 2, 3), ("dall", 3), ("drel", 1, 0),
        ("dsend", 2, 0), ("drel", 1, 1), ("trel", 2, 2), ("uall", 1), ("uall", 2), ("trel", 1, 0), ("uall", 3),
        ("uall", 0), ("trel", 2, 1), ("hid", 2), ("proj", 3, 2), ("ddiag", 1, 0), ("proj", 0, 2), ("hid", 1),
        ("ddiag", 1, 1), ("tsend", 2, 0), ("sum", 2, 3), ("proj", 3, 1), ("sum", 1, 3), ("sum", 2, 0), ("trel", 3, 1),
        ("trel", 3, 3), ("trel", 3, 2), ("hid", 0), ("drel", 2, 0), ("dall", 1), ("proj", 1, 2), ("trel", 3, 0),
        ("sum", 2, 1), ("hid", 3), ("drel", 2, 1), ("proj", 3, 3), ("sum", 3, 3), ("ddiag", 2, 0), ("proj", 1, 3),
        ("ddiag", 2, 1), ("sum", 3, 1), ("proj", 0, 3), ("proj", 0, 1), ("sum", 3, 0), ("dall", 2), ("proj", 2, 3),
        ("sum", 3, 2), ("sum", 1, 0), ("proj", 3, 0), ("proj", 1, 1), ("proj", 2, 2), ("proj", 2, 1), ("sum", 2, 2),
        ("sum", 1, 1), ("proj", 2, 0), ("sum", 1, 2), ("proj", 1, 0), ("proj", 0, 0), ("sum", 0, 0), ("sum", 0, 2),
        ("sum", 0, 3), ("sum", 0, 1),
    ],
    1: [
        ("uown",), ("usend", 3, 1), ("usend", 2, 1), ("usend", 3, 0), ("usend", 2, 0), ("usend", 0, 1),
        ("usend", 0, 0), ("norm",), ("tsend", 0, 0), ("down_own",), ("urel", 2, 1), ("tsend", 1, 1), ("dsend", 0, 1),
        ("tsend", 3, 1), ("tsend", 0, 1), ("urel", 0, 1), ("tsend", 2, -1), ("urel", 2, 0), ("tsend", 2, 0),
        ("tsend", 2, 1), ("tsend", 1, -1), ("urel", 0, 0), ("udiag", 2, 1), ("udiag", 0, 1), ("drel", 0, 0),
        ("trel", 2, 1), ("tsend", 3, -1), ("dsend", 0, 0), ("urel", 3, 0), ("ddiag", 1, 0), ("tsend", 3, 0),
        ("udiag", 1, 0), ("urel", 3, 1), ("udiag", 1, 1), ("trel", 2, 3), ("tsend", 1, 0), ("drel", 3, 1),
        ("udiag", 0, 0), ("trel", 2, 0), ("trel", 0, 3), ("trel", 0, 2), ("tsend", 0, -1), ("trel", 0, 1),
        ("uall", 1), ("udiag", 2, 0), ("trel", 2, 2), ("ddiag", 1, 1), ("dsend", 2, 0), ("uall", 2), ("trel", 0, 0),
        ("dall", 1), ("ddiag", 0, 0), ("dsend", 3, 0), ("udiag", 3, 0), ("trel", 3, 2), ("ddiag", 3, 1),
        ("udiag", 3, 1), ("trel", 3, 3), ("drel", 3, 0), ("drel", 0, 1), ("trel", 3, 1), ("uall", 0), ("dsend", 2, 1),
        ("uall", 3), ("hid", 1), ("hid", 2), ("trel", 3, 0), ("ddiag", 3, 0), ("hid", 3), ("dsend", 3, 1),
        ("ddiag", 0, 1), ("drel", 2, 0), ("drel", 2, 1), ("dall", 3), ("proj", 3, 2), ("proj", 1, 3), ("proj", 1, 2),
        ("hid", 0), ("proj", 3, 3), ("sum", 2, 3), ("proj", 1, 1), ("proj", 3, 0), ("ddiag", 2, 1), ("sum", 2, 1),
        ("dall", 0), ("proj", 0, 0), ("ddiag", 2, 0), ("proj", 3, 1), ("proj", 0, 2), ("proj", 0, 1), ("sum", 3, 3),
        ("sum", 3, 1), ("proj", 0, 3), ("dall", 2), ("proj", 2, 3), ("proj", 2, 2), ("sum", 0, 0), ("sum", 3, 0),
        ("proj", 1, 0), ("proj", 2, 0), ("sum", 0, 2), ("sum", 3, 2), ("sum", 2, 0), ("sum", 0, 3), ("proj", 2, 1),
        ("sum", 0, 1), ("sum", 2, 2), ("sum", 1, 3), ("sum", 1, 0), ("sum", 1, 1), ("sum", 1, 2),
    ],
}


def kernel(Z, X, Y, C, tok, gain, up, down, out,
           tokb, upb, downb, tokg, upg, downg, hid, part, cin, zin, zout,
           in_s, wz_s, wz_r, wx_s, wx_r, wy_s, wy_r, wd_s, wd_r,
           t_s, t_r, tc_s, tc_r, rc_s, rc_r, rz_s, rz_r):
    T, D = tok.shape
    F = Z * X
    Dl = up.shape[0]
    B = upg.shape[2]
    fs, tp = lax.axis_index("fs"), lax.axis_index("tp")
    z, x = fs // X, fs % X
    y, c = tp // C, tp % C
    ox, oy, oc = X - 1 - x, Y - 1 - y, C - 1 - c
    low = z < Z // 2
    p = jnp.where(low, z, Z - 1 - z)
    side = jnp.where(low, 0, 1)

    def plane(q):
        return jnp.where(low, q, Z - 1 - q)

    def dev(zz=z, xx=x, yy=y, cc=c):
        return {"fs": zz * X + xx, "tp": yy * C + cc}

    def rcopy(src, dst, ss, rs, device):
        return pltpu.make_async_remote_copy(
            src_ref=src, dst_ref=dst, send_sem=ss, recv_sem=rs,
            device_id=device, device_id_type=MESH)

    def rows(start, size):
        return pl.ds(pl.multiple_of(start, size), size)

    barrier = pltpu.get_barrier_semaphore()
    peers = [dev(zz=(z + k) % Z) for k in range(1, Z)]
    peers += [dev(xx=ox), dev(yy=oy), dev(cc=oc)]
    for peer in peers:
        pl.semaphore_signal(barrier, inc=1, device_id=peer, device_id_type=MESH)

    loads = [
        pltpu.make_async_copy(up, upb, in_s.at[0]),
        pltpu.make_async_copy(tok, tokb, in_s.at[1]),
        pltpu.make_async_copy(down, downb, in_s.at[2]),
        pltpu.make_async_copy(up.at[:, rows(z * B, B)], upg.at[y, rows(fs * Dl, Dl)], in_s.at[3]),
        pltpu.make_async_copy(down.at[rows(z * B, B)], downg.at[fs, rows(y * B, B)], in_s.at[4]),
    ]
    for load in loads:
        load.start()
    loads[0].wait()
    loads[3].wait()
    pl.semaphore_wait(barrier, len(peers))

    def normalize():
        loads[1].wait()
        RB = 32

        @pl.loop(0, T // RB)
        def _(i):
            v = tokb[rows(i * RB, RB), :].astype(f32)
            ms = jnp.mean(v * v, axis=-1, keepdims=True)
            tokg[z, rows(c * T + i * RB, RB), :] = (v * lax.rsqrt(ms + epsilon) * gain[...]).astype(bf16)

        loads[2].wait()
        loads[4].wait()

    def piece(zz, xx, yy, k, half):
        f = zz * X + xx
        if k == 0:
            return upg.at[yy, rows(f * Dl + half * (Dl // 2), Dl // 2)]
        return downg.at[f, rows(yy * B + half * (B // 2), B // 2)]

    def own_piece(zz, k, half):
        if k == 0:
            return upb.at[rows(half * (Dl // 2), Dl // 2), rows(zz * B, B)]
        return downb.at[rows(zz * B + half * (B // 2), B // 2)]

    def wz(q, k, half):
        zz = plane(q)
        return rcopy(own_piece(zz, k, half), piece(z, x, y, k, half),
                     wz_s.at[k, zz, half], wz_r.at[k, z, half], dev(zz=zz))

    def wz_recv(q, k, half):
        zz = plane(q)
        ref = piece(zz, x, y, k, half)
        return rcopy(ref, ref, wz_s.at[k, zz, half], wz_r.at[k, zz, half], dev(zz=zz))

    def wx(q, k, half, xx=x):
        zz = plane(q)
        ref = piece(zz, xx, y, k, half)
        return rcopy(ref, ref, wx_s.at[k, zz, half], wx_r.at[k, zz, half], dev(xx=ox))

    def wy(q, k, half, yy=y):
        zz = plane(q)
        ref = piece(zz, x, yy, k, half)
        return rcopy(ref, ref, wy_s.at[k, zz, half], wy_r.at[k, zz, half], dev(yy=oy))

    def wd(q, k, half):
        zz = plane(q)
        ref = piece(zz, ox, y, k, 0) if half == 0 else piece(zz, x, oy, k, 1)
        to = dev(yy=oy) if half == 0 else dev(xx=ox)
        return rcopy(ref, ref, wd_s.at[k, zz, half], wd_r.at[k, zz, half], to)

    def wd_recv(q, k, half):
        zz = plane(q)
        ref = piece(zz, ox, oy, k, half)
        return rcopy(ref, ref, wd_s.at[k, zz, half], wd_r.at[k, zz, half], dev(yy=oy))

    TC = T // CUTS

    def tok_z(g, cut, way):
        gg = plane(g)
        ref = tokg.at[gg, rows(c * T + cut * TC, TC)]
        to = jnp.where(low, z + way, z - way)
        return rcopy(ref, ref, t_s.at[(way + 1) // 2, gg, cut], t_r.at[gg, cut], dev(zz=to))

    def tok_c(g, cut, cc=c):
        gg = plane(g)
        ref = tokg.at[gg, rows(cc * T + cut * TC, TC)]
        return rcopy(ref, ref, tc_s.at[gg, cut], tc_r.at[gg, cut], dev(cc=oc))

    NB = min(B, 512)

    def compute(g):
        gg = plane(g)
        for yy in range(Y):
            for j in range(B // NB):
                h = jnp.dot(tokg[gg], upg[yy, :, rows(j * NB, NB)], preferred_element_type=f32)
                h = jnp.maximum(h, 0.0)
                hid[gg, :, rows(yy * B + j * NB, NB)] = (h * h).astype(bf16)

    def sum_c(gg, f):
        return rcopy(part.at[gg, f, oc], cin.at[gg, f], rc_s.at[gg, f], rc_r.at[gg, f], dev(cc=oc))

    def project(q, g):
        gg = plane(g)

        @pl.loop(0, X)
        def _(xx):
            f = plane(q) * X + xx
            v = jnp.dot(hid[gg], downg[f], preferred_element_type=f32).astype(bf16)
            for cc in range(C):
                part[gg, f, cc] = v[cc * T:(cc + 1) * T]
            sum_c(gg, f).start()

    def sum_z(gg, f, way):
        to = jnp.where(low, z + way, z - way)
        at = side if way > 0 else 1 - side
        return rcopy(zout.at[gg, f], zin.at[at, gg, f], rz_s.at[gg, f], rz_r.at[at, gg, f], dev(zz=to))

    def step(me, g, q):
        gg = plane(g)

        @pl.loop(0, X)
        def _(xx):
            f = plane(q) * X + xx
            sum_c(gg, f).wait_recv()
            acc = part[gg, f, c].astype(f32) + cin[gg, f].astype(f32)
            if me > 0 and g >= me:
                sum_z(gg, f, 1).wait_recv()
                acc = acc + zin[side, gg, f].astype(f32)
            if g <= me:
                sum_z(gg, f, -1).wait_recv()
                acc = acc + zin[1 - side, gg, f].astype(f32)
            if g == me:
                out[:, rows(f * Dl, Dl)] = acc.astype(bf16)
            else:
                zout[gg, f] = acc.astype(bf16)
                sum_z(gg, f, 1 if g > me else -1).start()

    def run(me, op, *args):
        k = 0 if op[0] == "u" else 1
        if op == "norm":
            normalize()
        elif op == "uown" or op == "down_own":
            for half in range(2):
                wx(me, k, half).start()
                wy(me, k, half).start()
        elif op == "usend" or op == "dsend":
            wz(args[0], k, args[1]).start()
        elif op == "urel" or op == "drel":
            q, half = args
            wz_recv(q, k, half).wait_recv()
            wx(q, k, half).start()
            wy(q, k, half).start()
        elif op == "udiag" or op == "ddiag":
            q, half = args
            if half == 0:
                wx(q, k, 0, ox).wait_recv()
            else:
                wy(q, k, 1, oy).wait_recv()
            wd(q, k, half).start()
        elif op == "uall" or op == "dall":
            q = args[0]
            wx(q, k, 1, ox).wait_recv()
            wy(q, k, 0, oy).wait_recv()
            for half in range(2):
                wd_recv(q, k, half).wait_recv()
        elif op == "tsend":
            cut, way = args
            if way == 0:
                tok_c(me, cut).start()
            else:
                tok_z(me, cut, way).start()
        elif op == "trel":
            g, cut = args
            tok_z(g, cut, 1 if g < me else -1).wait_recv()
            if me > 0:
                tok_z(g, cut, 1 if g < me else -1).start()
            tok_c(g, cut).start()
        elif op == "hid":
            for cut in range(CUTS):
                tok_c(args[0], cut, oc).wait_recv()
            compute(args[0])
        elif op == "proj":
            project(*args)
        elif op == "sum":
            step(me, *args)

    def drain(me):
        for q in range(Z):
            for k in range(2):
                for half in range(2):
                    if q != me:
                        wz(q, k, half).wait_send()
                    wx(q, k, half).wait_send()
                    wy(q, k, half).wait_send()
                    wd(q, k, half).wait_send()
            for cut in range(CUTS):
                tok_c(q, cut).wait_send()
                if q <= me:
                    tok_z(q, cut, 1).wait_send()
                if q >= me and me > 0:
                    tok_z(q, cut, -1).wait_send()

    for me in range(Z // 2):
        @pl.when(p == me)
        def _(me=me):
            for item in PROGRAM[me]:
                run(me, *item)
            drain(me)

    @pl.loop(0, F)
    def _(f):
        @pl.loop(0, Z)
        def _(gg):
            sum_c(gg, f).wait_send()

            @pl.when(gg != z)
            def _():
                sum_z(gg, f, 1).wait_send()


def solution(mesh):
    n_fs, n_tp = mesh.shape["fs"], mesh.shape["tp"]
    X = 2 ** (int(math.log2(n_fs)) // 2)
    Z = n_fs // X
    C = 2
    Y = n_tp // C
    placed = (P(("fs", "tp"), None), P(), P("fs", "tp"), P("tp", "fs"))

    def on_device(tokens, norm_gain, up_weight, down_weight):
        T, D = tokens.shape
        Dl, FFl = up_weight.shape
        B = FFl // Z
        if X != 2 or Y != 2 or Z != 4 or Z * X != n_fs or Dl % 256 or B % 256 or T % (16 * CUTS):
            return plain(tokens, norm_gain, up_weight, down_weight)
        F = Z * X
        dma = pltpu.SemaphoreType.DMA
        vm = pl.BlockSpec(memory_space=pltpu.VMEM)
        hbm = pl.BlockSpec(memory_space=pltpu.HBM)
        return pl.pallas_call(
            functools.partial(kernel, Z, X, Y, C),
            out_shape=jax.ShapeDtypeStruct((T, D), bf16),
            in_specs=[hbm, vm, hbm, hbm],
            out_specs=vm,
            scratch_shapes=[
                pltpu.VMEM((T, D), bf16),
                pltpu.VMEM((Dl, FFl), bf16),
                pltpu.VMEM((FFl, Dl), bf16),
                pltpu.VMEM((Z, C * T, D), bf16),
                pltpu.VMEM((Y, D, B), bf16),
                pltpu.VMEM((F, Y * B, Dl), bf16),
                pltpu.VMEM((Z, C * T, Y * B), bf16),
                pltpu.VMEM((Z, F, C, T, Dl), bf16),
                pltpu.VMEM((Z, F, T, Dl), bf16),
                pltpu.VMEM((2, Z, F, T, Dl), bf16),
                pltpu.VMEM((Z, F, T, Dl), bf16),
                dma((5,)),
                *[dma((2, Z, 2)) for _ in range(8)],
                dma((2, Z, CUTS)), *[dma((Z, CUTS)) for _ in range(3)],
                dma((Z, F)), dma((Z, F)), dma((Z, F)), dma((2, Z, F)),
            ],
            compiler_params=pltpu.CompilerParams(
                collective_id=0, has_side_effects=True, vmem_limit_bytes=53 * 2**20),
        )(tokens, norm_gain.reshape(1, D), up_weight, down_weight)

    return jax.shard_map(
        on_device, mesh=mesh, in_specs=placed, out_specs=P(("fs", "tp"), None), check_vma=False)
```

time: 109 us -> 105 us (0.963)
  Pallas kernels: 107 us -> 103 us
    pallas_call x1, Pallas kernels: 107 us -> 103 us  [on_device(): pl.pallas_call(functools.partial(kernel, Z, X, Y, C), out_shape=jax.Shape...]
where the time goes in v4:
time: 105 us
  Pallas kernels  103 us (98%)
  local copies, waits for them, and re-layouts  1.49 us (1%)
    pallas_call x1, Pallas kernels, on_device(): pl.pallas_call(functools.partial(kernel, Z, X, Y, C), out_shape=jax.Shape...  103 us

profile of v4, /device:TPU:0, one launch (start us, length us, event | category | flops | bytes accessed | tf_op | source)
XLA Modules:
  0.0 104.7 jit_solution(2948883341820986632)
XLA Ops:
  0.0 0.0 copy-start
  0.0 0.7 copy-done
  0.7 103.2 %shard_map.46 = bf16[128,2048]{1,0:T(8,128)(2,1)S(1)} custom-call(bf16[128,2048]{1,0:T(8,128)(2,1)} %tok.1, f32[1,2048]{1,0:T(1,128)S(1)} %bitcast.1, bf16[256,2048]{1,0:T(8,128)(2,1)} %up.1, bf16[2048,256]{1,0:T(8,128)(2,1)} %down.1), custom_call_target="tpu_custom_call" | custom-call | tf_op jit(solution)/shard_map/pallas_call | solution.py:339
  103.9 0.8 copy.6
Async XLA Ops:
  0.0 0.7 copy-start

commit v5 on v4

v5 whole, which is shorter than its diff:
```python
import functools
import math

import jax
import jax.numpy as jnp
from jax import lax
from jax.experimental import pallas as pl
from jax.experimental.pallas import tpu as pltpu
from jax.sharding import PartitionSpec as P

epsilon = 1e-06
MESH = pl.DeviceIdType.MESH
CUTS = 4
f32, bf16 = jnp.float32, jnp.bfloat16


def plain(tokens, norm_gain, up_weight, down_weight):
    values = tokens.astype(f32)
    mean_square = jnp.mean(values * values, axis=-1, keepdims=True)
    normed = (values * lax.rsqrt(mean_square + epsilon) * norm_gain).astype(bf16)
    up_whole = lax.all_gather(up_weight, "fs", axis=0, tiled=True)
    rows = lax.all_gather(normed, "tp", axis=0, tiled=True)
    preact = jnp.dot(rows, up_whole, preferred_element_type=f32)
    hidden = jnp.square(jnp.maximum(preact, 0.0)).astype(bf16)
    down_whole = lax.all_gather(down_weight, "fs", axis=1, tiled=True)
    partial_value = jnp.dot(hidden, down_whole, preferred_element_type=f32).astype(bf16)
    return lax.psum_scatter(partial_value, "tp", scatter_dimension=0, tiled=True)


PROGRAM = {
    0: [
        ("usend", 1, 0), ("usend", 3, 1), ("uown",), ("norm",), ("usend", 2, 1), ("down_own",), ("usend", 3, 0),
        ("urel", 3, 1), ("tsend", 0, 1), ("tsend", 3, 1), ("usend", 1, 1), ("urel", 2, 1), ("tsend", 0, 0),
        ("dsend", 1, 0), ("usend", 2, 0), ("dsend", 1, 1), ("dsend", 2, 1), ("tsend", 1, 1), ("urel", 3, 0),
        ("urel", 1, 0), ("urel", 1, 1), ("trel", 1, 1), ("drel", 1, 1), ("ddiag", 0, 0), ("urel", 2, 0),
        ("udiag", 1, 1), ("udiag", 0, 0), ("drel", 1, 0), ("dsend", 2, 0), ("tsend", 2, 1), ("udiag", 2, 1),
        ("udiag", 3, 1), ("udiag", 3, 0), ("dsend", 3, 0), ("udiag", 1, 0), ("udiag", 0, 1), ("ddiag", 1, 1),
        ("ddiag", 1, 0), ("ddiag", 0, 1), ("udiag", 2, 0), ("dsend", 3, 1), ("uall", 1), ("uall", 3), ("trel", 1, 3),
        ("trel", 1, 0), ("trel", 1, 2), ("trel", 3, 3), ("drel", 3, 1), ("uall", 2), ("dall", 0), ("uall", 0),
        ("drel", 3, 0), ("hid", 1), ("trel", 3, 0), ("dall", 1), ("proj", 1, 1), ("trel", 3, 2), ("proj", 0, 1),
        ("trel", 3, 1), ("ddiag", 3, 1), ("sum", 1, 0), ("hid", 3), ("ddiag", 3, 0), ("sum", 1, 1), ("proj", 1, 3),
        ("drel", 2, 1), ("proj", 0, 3), ("sum", 3, 0), ("drel", 2, 0), ("sum", 3, 1), ("dall", 3), ("proj", 3, 1),
        ("tsend", 2, 0), ("trel", 2, 3), ("proj", 3, 3), ("sum", 3, 3), ("trel", 2, 1), ("tsend", 1, 0),
        ("ddiag", 2, 1), ("trel", 2, 2), ("trel", 2, 0), ("ddiag", 2, 0), ("sum", 1, 3), ("hid", 2), ("proj", 3, 2),
        ("sum", 2, 3), ("tsend", 3, 0), ("dall", 2), ("proj", 0, 2), ("sum", 2, 0), ("proj", 2, 2), ("proj", 2, 3),
        ("hid", 0), ("proj", 3, 0), ("sum", 3, 2), ("sum", 2, 2), ("proj", 1, 2), ("sum", 2, 1), ("proj", 2, 1),
        ("proj", 0, 0), ("sum", 0, 0), ("sum", 0, 3), ("proj", 1, 0), ("proj", 2, 0), ("sum", 1, 2), ("sum", 0, 2),
        ("sum", 0, 1),
    ],
    1: [
        ("uown",), ("usend", 3, 1), ("usend", 0, 0), ("usend", 3, 0), ("usend", 2, 1), ("norm",), ("tsend", 1, -1),
        ("down_own",), ("urel", 3, 1), ("trel", 0, 0), ("usend", 0, 1), ("urel", 0, 0), ("udiag", 1, 1),
        ("urel", 2, 1), ("dsend", 0, 1), ("dsend", 0, 0), ("udiag", 3, 1), ("udiag", 1, 0), ("tsend", 0, -1),
        ("ddiag", 1, 1), ("trel", 0, 3), ("tsend", 3, 1), ("trel", 3, 0), ("urel", 0, 1), ("usend", 2, 0),
        ("ddiag", 1, 0), ("trel", 2, 3), ("tsend", 3, 0), ("drel", 0, 1), ("tsend", 3, -1), ("drel", 0, 0),
        ("udiag", 0, 0), ("trel", 3, 3), ("trel", 0, 1), ("urel", 3, 0), ("trel", 0, 2), ("udiag", 0, 1),
        ("urel", 2, 0), ("tsend", 2, -1), ("tsend", 1, 1), ("trel", 3, 1), ("tsend", 0, 1), ("dsend", 3, 1),
        ("udiag", 3, 0), ("drel", 3, 1), ("udiag", 2, 0), ("udiag", 2, 1), ("ddiag", 0, 0), ("trel", 3, 2),
        ("dsend", 3, 0), ("tsend", 1, 0), ("uall", 1), ("ddiag", 0, 1), ("tsend", 2, 1), ("trel", 2, 0),
        ("tsend", 0, 0), ("uall", 2), ("uall", 3), ("dall", 1), ("drel", 3, 0), ("trel", 2, 1), ("uall", 0),
        ("dsend", 2, 1), ("tsend", 2, 0), ("hid", 3), ("hid", 0), ("dall", 0), ("ddiag", 3, 0), ("proj", 0, 0),
        ("ddiag", 3, 1), ("dsend", 2, 0), ("proj", 0, 3), ("proj", 1, 3), ("trel", 2, 2), ("hid", 1), ("dall", 3),
        ("drel", 2, 1), ("proj", 0, 1), ("sum", 3, 0), ("proj", 3, 3), ("drel", 2, 0), ("sum", 3, 1), ("hid", 2),
        ("proj", 3, 0), ("sum", 3, 3), ("ddiag", 2, 0), ("ddiag", 2, 1), ("sum", 0, 3), ("proj", 3, 2),
        ("proj", 1, 2), ("proj", 0, 2), ("sum", 0, 0), ("sum", 2, 3), ("dall", 2), ("proj", 2, 0), ("proj", 1, 0),
        ("proj", 2, 3), ("sum", 2, 0), ("sum", 0, 2), ("proj", 2, 2), ("sum", 3, 2), ("sum", 2, 2), ("proj", 1, 1),
        ("proj", 2, 1), ("proj", 3, 1), ("sum", 0, 1), ("sum", 2, 1), ("sum", 1, 0), ("sum", 1, 3), ("sum", 1, 1),
        ("sum", 1, 2),
    ],
}


def kernel(Z, X, Y, C, tok, gain, up, down, out,
           tokb, upb, downb, tokg, upg, downg, hid, part, cin, zin, zout,
           in_s, wz_s, wx_s, wy_s, wd_s, t_s, tc_s, rc_s, rz_s,
           wz_r, wx_r, wy_r, all_r, t_r, tc_r, rc_r, rz_r):
    T, D = tok.shape
    F = Z * X
    Dl = up.shape[0]
    B = upg.shape[2]
    fs, tp = lax.axis_index("fs"), lax.axis_index("tp")
    z, x = fs // X, fs % X
    y, c = tp // C, tp % C
    ox, oy, oc = X - 1 - x, Y - 1 - y, C - 1 - c
    low = z < Z // 2
    p = jnp.where(low, z, Z - 1 - z)

    def plane(q):
        return jnp.where(low, q, Z - 1 - q)

    def dev(zz=z, xx=x, yy=y, cc=c):
        return {"fs": zz * X + xx, "tp": yy * C + cc}

    def rcopy(src, dst, ss, rs, device):
        return pltpu.make_async_remote_copy(
            src_ref=src, dst_ref=dst, send_sem=ss, recv_sem=rs,
            device_id=device, device_id_type=MESH)

    def rows(start, size):
        return pl.ds(pl.multiple_of(start, size), size)

    barrier = pltpu.get_barrier_semaphore()
    peers = [dev(zz=(z + k) % Z) for k in range(1, Z)]
    peers += [dev(xx=ox), dev(yy=oy), dev(cc=oc)]
    for peer in peers:
        pl.semaphore_signal(barrier, inc=1, device_id=peer, device_id_type=MESH)

    loads = [
        pltpu.make_async_copy(up, upb, in_s.at[0]),
        pltpu.make_async_copy(up.at[:, rows(z * B, B)], upg.at[y, rows(fs * Dl, Dl)], in_s.at[1]),
        pltpu.make_async_copy(tok, tokb, in_s.at[2]),
        pltpu.make_async_copy(down, downb, in_s.at[3]),
        pltpu.make_async_copy(down.at[rows(z * B, B)], downg.at[fs, rows(y * B, B)], in_s.at[4]),
    ]
    for load in loads[:3]:
        load.start()
    loads[0].wait()
    for load in loads[3:]:
        load.start()
    loads[1].wait()
    pl.semaphore_wait(barrier, len(peers))

    def normalize():
        loads[2].wait()
        RB = 32

        @pl.loop(0, T // RB)
        def _(i):
            v = tokb[rows(i * RB, RB), :].astype(f32)
            ms = jnp.mean(v * v, axis=-1, keepdims=True)
            tokg[z, rows(c * T + i * RB, RB), :] = (v * lax.rsqrt(ms + epsilon) * gain[...]).astype(bf16)

        loads[3].wait()
        loads[4].wait()

    def piece(zz, xx, yy, k, half):
        f = zz * X + xx
        if k == 0:
            return upg.at[yy, rows(f * Dl + half * (Dl // 2), Dl // 2)]
        return downg.at[f, rows(yy * B + half * (B // 2), B // 2)]

    def own_piece(zz, k, half):
        if k == 0:
            return upb.at[rows(half * (Dl // 2), Dl // 2), rows(zz * B, B)]
        return downb.at[rows(zz * B + half * (B // 2), B // 2)]

    def wz(q, k, half):
        zz = plane(q)
        return rcopy(own_piece(zz, k, half), piece(z, x, y, k, half),
                     wz_s.at[0], wz_r.at[k, z, half], dev(zz=zz))

    def wz_recv(q, k, half):
        zz = plane(q)
        ref = piece(zz, x, y, k, half)
        return rcopy(ref, ref, wz_s.at[0], wz_r.at[k, zz, half], dev(zz=zz))

    def wx(q, k, half, xx=x):
        zz = plane(q)
        ref = piece(zz, xx, y, k, half)
        rs = wx_r.at[k, zz] if half == 0 else all_r.at[k, zz]
        return rcopy(ref, ref, wx_s.at[0], rs, dev(xx=ox))

    def wy(q, k, half, yy=y):
        zz = plane(q)
        ref = piece(zz, x, yy, k, half)
        rs = wy_r.at[k, zz] if half == 1 else all_r.at[k, zz]
        return rcopy(ref, ref, wy_s.at[0], rs, dev(yy=oy))

    def wd(q, k, half):
        zz = plane(q)
        ref = piece(zz, ox, y, k, 0) if half == 0 else piece(zz, x, oy, k, 1)
        to = dev(yy=oy) if half == 0 else dev(xx=ox)
        return rcopy(ref, ref, wd_s.at[0], all_r.at[k, zz], to)

    def rest_recv(q, k):
        zz = plane(q)
        ref = upg.at[y, pl.ds(0, 2 * Dl)] if k == 0 else downg.at[zz * X]
        return rcopy(ref, ref, wd_s.at[0], all_r.at[k, zz], dev(yy=oy))

    TC = T // CUTS

    def tok_z(g, cut, way):
        gg = plane(g)
        ref = tokg.at[gg, rows(c * T + cut * TC, TC)]
        to = jnp.where(low, z + way, z - way)
        return rcopy(ref, ref, t_s.at[0], t_r.at[gg, cut], dev(zz=to))

    def tok_c(g, cut, cc=c):
        gg = plane(g)
        ref = tokg.at[gg, rows(cc * T + cut * TC, TC)]
        return rcopy(ref, ref, tc_s.at[0], tc_r.at[gg], dev(cc=oc))

    NB = min(B, 512)

    def compute(g):
        gg = plane(g)
        for yy in range(Y):
            for j in range(B // NB):
                h = jnp.dot(tokg[gg], upg[yy, :, rows(j * NB, NB)], preferred_element_type=f32)
                h = jnp.maximum(h, 0.0)
                hid[gg, :, rows(yy * B + j * NB, NB)] = (h * h).astype(bf16)

    def sum_c(gg, f):
        return rcopy(part.at[gg, f, oc], cin.at[gg, f], rc_s.at[0], rc_r.at[gg, f], dev(cc=oc))

    def project(q, g):
        gg = plane(g)

        @pl.loop(0, X)
        def _(xx):
            f = plane(q) * X + xx
            v = jnp.dot(hid[gg], downg[f], preferred_element_type=f32).astype(bf16)
            for cc in range(C):
                part[gg, f, cc] = v[cc * T:(cc + 1) * T]
            sum_c(gg, f).start()

    def sum_z(me, g, f, way, slot):
        to = jnp.where(low, z + way, z - way)
        return rcopy(zout.at[plane(g), f], zin.at[slot, f], rz_s.at[0], rz_r.at[slot, f], dev(zz=to))

    def step(me, g, q):
        gg = plane(g)

        @pl.loop(0, X)
        def _(xx):
            f = plane(q) * X + xx
            sum_c(gg, f).wait_recv()
            acc = part[gg, f, c].astype(f32) + cin[gg, f].astype(f32)
            slots = ([g] if me > 0 and g >= me else []) + ([g and Z] if g <= me else [])
            for slot in slots:
                sum_z(me, g, f, 1, slot).wait_recv()
                acc = acc + zin[slot, f].astype(f32)
            if g == me:
                out[:, rows(f * Dl, Dl)] = acc.astype(bf16)
            else:
                zout[gg, f] = acc.astype(bf16)
                if g < me:
                    sum_z(me, g, f, -1, 0).start()
                else:
                    sum_z(me, g, f, 1, g if me == 0 else (Z - 1 - g) and Z).start()

    def run(me, op, *args):
        k = 0 if op[0] == "u" else 1
        if op == "norm":
            normalize()
        elif op == "uown" or op == "down_own":
            for half in range(2):
                wx(me, k, half).start()
                wy(me, k, half).start()
        elif op == "usend" or op == "dsend":
            wz(args[0], k, args[1]).start()
        elif op == "urel" or op == "drel":
            q, half = args
            wz_recv(q, k, half).wait_recv()
            wx(q, k, half).start()
            wy(q, k, half).start()
        elif op == "udiag" or op == "ddiag":
            q, half = args
            if half == 0:
                wx(q, k, 0, ox).wait_recv()
            else:
                wy(q, k, 1, oy).wait_recv()
            wd(q, k, half).start()
        elif op == "uall" or op == "dall":
            q = args[0]
            rest_recv(q, k).wait_recv()
        elif op == "tsend":
            cut, way = args
            if way == 0:
                tok_c(me, cut).start()
            else:
                tok_z(me, cut, way).start()
        elif op == "trel":
            g, cut = args
            tok_z(g, cut, 1 if g < me else -1).wait_recv()
            if me > 0:
                tok_z(g, cut, 1 if g < me else -1).start()
            tok_c(g, cut).start()
        elif op == "hid":
            ref = tokg.at[plane(args[0]), rows(oc * T, T)]
            rcopy(ref, ref, tc_s.at[0], tc_r.at[plane(args[0])], dev(cc=oc)).wait_recv()
            compute(args[0])
        elif op == "proj":
            project(*args)
        elif op == "sum":
            step(me, *args)

    def sent(ref, sem):
        rcopy(ref, ref, sem.at[0], rc_r.at[0, 0], dev(cc=oc)).wait_send()

    def drain(me):
        sent(upg.at[:, pl.ds(0, (Z - 1) * Dl)], wz_s)
        sent(upg.at[0], wx_s)
        sent(upg.at[0], wy_s)
        sent(upg.at[0], wd_s)
        sent(tokg.at[0, pl.ds(0, T)] if me == 0 else upg.at[:, pl.ds(0, 5 * Dl)], t_s)
        sent(tokg.at[pl.ds(0, 2)], tc_s)
        sent(zout.at[pl.ds(0, Z - 1)], rz_s)
        sent(zout, rc_s)

    for me in range(Z // 2):
        @pl.when(p == me)
        def _(me=me):
            for item in PROGRAM[me]:
                run(me, *item)
            drain(me)


def solution(mesh):
    n_fs, n_tp = mesh.shape["fs"], mesh.shape["tp"]
    X = 2 ** (int(math.log2(n_fs)) // 2)
    Z = n_fs // X
    C = 2
    Y = n_tp // C
    placed = (P(("fs", "tp"), None), P(), P("fs", "tp"), P("tp", "fs"))

    def on_device(tokens, norm_gain, up_weight, down_weight):
        T, D = tokens.shape
        Dl, FFl = up_weight.shape
        B = FFl // Z
        if X != 2 or Y != 2 or Z != 4 or Z * X != n_fs or Dl % 256 or B % 256 or T % (16 * CUTS):
            return plain(tokens, norm_gain, up_weight, down_weight)
        F = Z * X
        dma = pltpu.SemaphoreType.DMA
        vm = pl.BlockSpec(memory_space=pltpu.VMEM)
        hbm = pl.BlockSpec(memory_space=pltpu.HBM)
        return pl.pallas_call(
            functools.partial(kernel, Z, X, Y, C),
            out_shape=jax.ShapeDtypeStruct((T, D), bf16),
            in_specs=[hbm, vm, hbm, hbm],
            out_specs=vm,
            scratch_shapes=[
                pltpu.VMEM((T, D), bf16),
                pltpu.VMEM((Dl, FFl), bf16),
                pltpu.VMEM((FFl, Dl), bf16),
                pltpu.VMEM((Z, C * T, D), bf16),
                pltpu.VMEM((Y, D, B), bf16),
                pltpu.VMEM((F, Y * B, Dl), bf16),
                pltpu.VMEM((Z, C * T, Y * B), bf16),
                pltpu.VMEM((Z, F, C, T, Dl), bf16),
                pltpu.VMEM((Z, F, T, Dl), bf16),
                pltpu.VMEM((Z + 1, F, T, Dl), bf16),
                pltpu.VMEM((Z, F, T, Dl), bf16),
                dma((5,)),
                *[dma((1,)) for _ in range(8)],
                dma((2, Z, 2)), dma((2, Z)), dma((2, Z)), dma((2, Z)),
                dma((Z, CUTS)), dma((Z,)), dma((Z, F)), dma((Z + 1, F)),
            ],
            compiler_params=pltpu.CompilerParams(
                collective_id=0, has_side_effects=True, vmem_limit_bytes=53 * 2**20),
        )(tokens, norm_gain.reshape(1, D), up_weight, down_weight)

    return jax.shard_map(
        on_device, mesh=mesh, in_specs=placed, out_specs=P(("fs", "tp"), None), check_vma=False)
```

time: 105 us -> 102 us (0.971)
  Pallas kernels: 103 us -> 100 us
    pallas_call x1, Pallas kernels: 103 us -> 100 us  [on_device(): pl.pallas_call(functools.partial(kernel, Z, X, Y, C), out_shape=jax.Shape...]
where the time goes in v5:
time: 102 us
  Pallas kernels  100 us (98%)
  local copies, waits for them, and re-layouts  1.49 us (1%)
    pallas_call x1, Pallas kernels, on_device(): pl.pallas_call(functools.partial(kernel, Z, X, Y, C), out_shape=jax.Shape...  100 us

profile of v5, /device:TPU:0, one launch (start us, length us, event | category | flops | bytes accessed | tf_op | source)
XLA Modules:
  0.0 101.7 jit_solution(15567898410601240055)
XLA Ops:
  0.0 0.0 copy-start
  0.0 0.7 copy-done
  0.7 100.2 %shard_map.46 = bf16[128,2048]{1,0:T(8,128)(2,1)S(1)} custom-call(bf16[128,2048]{1,0:T(8,128)(2,1)} %tok.1, f32[1,2048]{1,0:T(1,128)S(1)} %bitcast.1, bf16[256,2048]{1,0:T(8,128)(2,1)} %up.1, bf16[2048,256]{1,0:T(8,128)(2,1)} %down.1), custom_call_target="tpu_custom_call" | custom-call | tf_op jit(solution)/shard_map/pallas_call | solution.py:327
  100.9 0.8 copy.6
Async XLA Ops:
  0.0 0.7 copy-start

commit v6 on v5

--- a/solution.py
+++ b/solution.py
@@ -29,49 +29,49 @@
 
 PROGRAM = {
     0: [
-        ("usend", 1, 0), ("usend", 3, 1), ("uown",), ("norm",), ("usend", 2, 1), ("down_own",), ("usend", 3, 0),
-        ("urel", 3, 1), ("tsend", 0, 1), ("tsend", 3, 1), ("usend", 1, 1), ("urel", 2, 1), ("tsend", 0, 0),
-        ("dsend", 1, 0), ("usend", 2, 0), ("dsend", 1, 1), ("dsend", 2, 1), ("tsend", 1, 1), ("urel", 3, 0),
-        ("urel", 1, 0), ("urel", 1, 1), ("trel", 1, 1), ("drel", 1, 1), ("ddiag", 0, 0), ("urel", 2, 0),
-        ("udiag", 1, 1), ("udiag", 0, 0), ("drel", 1, 0), ("dsend", 2, 0), ("tsend", 2, 1), ("udiag", 2, 1),
-        ("udiag", 3, 1), ("udiag", 3, 0), ("dsend", 3, 0), ("udiag", 1, 0), ("udiag", 0, 1), ("ddiag", 1, 1),
-        ("ddiag", 1, 0), ("ddiag", 0, 1), ("udiag", 2, 0), ("dsend", 3, 1), ("uall", 1), ("uall", 3), ("trel", 1, 3),
-        ("trel", 1, 0), ("trel", 1, 2), ("trel", 3, 3), ("drel", 3, 1), ("uall", 2), ("dall", 0), ("uall", 0),
-        ("drel", 3, 0), ("hid", 1), ("trel", 3, 0), ("dall", 1), ("proj", 1, 1), ("trel", 3, 2), ("proj", 0, 1),
-        ("trel", 3, 1), ("ddiag", 3, 1), ("sum", 1, 0), ("hid", 3), ("ddiag", 3, 0), ("sum", 1, 1), ("proj", 1, 3),
-        ("drel", 2, 1), ("proj", 0, 3), ("sum", 3, 0), ("drel", 2, 0), ("sum", 3, 1), ("dall", 3), ("proj", 3, 1),
-        ("tsend", 2, 0), ("trel", 2, 3), ("proj", 3, 3), ("sum", 3, 3), ("trel", 2, 1), ("tsend", 1, 0),
-        ("ddiag", 2, 1), ("trel", 2, 2), ("trel", 2, 0), ("ddiag", 2, 0), ("sum", 1, 3), ("hid", 2), ("proj", 3, 2),
-        ("sum", 2, 3), ("tsend", 3, 0), ("dall", 2), ("proj", 0, 2), ("sum", 2, 0), ("proj", 2, 2), ("proj", 2, 3),
-        ("hid", 0), ("proj", 3, 0), ("sum", 3, 2), ("sum", 2, 2), ("proj", 1, 2), ("sum", 2, 1), ("proj", 2, 1),
-        ("proj", 0, 0), ("sum", 0, 0), ("sum", 0, 3), ("proj", 1, 0), ("proj", 2, 0), ("sum", 1, 2), ("sum", 0, 2),
-        ("sum", 0, 1),
+        ("uown",), ("norm",), ("usend", 2, 1), ("usend", 1, 0), ("urel", 1, 1), ("dsend", 1, 1), ("usend", 3, 1),
+        ("tsend", 3, 1), ("down_own",), ("usend", 1, 1), ("usend", 3, 0), ("urel", 2, 0), ("urel", 3, 1),
+        ("urel", 1, 0), ("dsend", 2, 0), ("tsend", 1, 1), ("udiag", 0, 1), ("udiag", 0, 0), ("usend", 2, 0),
+        ("dsend", 3, 1), ("tsend", 2, 1), ("urel", 3, 0), ("udiag", 2, 0), ("udiag", 3, 1), ("ddiag", 0, 0),
+        ("tsend", 0, 0), ("urel", 2, 1), ("udiag", 1, 1), ("dsend", 1, 0), ("drel", 1, 1), ("udiag", 1, 0),
+        ("tsend", 1, 0), ("tsend", 0, 1), ("trel", 1, 2), ("udiag", 3, 0), ("trel", 1, 1), ("udiag", 2, 1),
+        ("dsend", 3, 0), ("ddiag", 0, 1), ("drel", 1, 0), ("tsend", 2, 0), ("tsend", 3, 0), ("ddiag", 1, 1),
+        ("dsend", 2, 1), ("uall", 1), ("uall", 3), ("trel", 1, 3), ("trel", 2, 2), ("uall", 2), ("trel", 1, 0),
+        ("drel", 3, 0), ("uall", 0), ("trel", 3, 3), ("dall", 0), ("ddiag", 1, 0), ("hid", 1), ("drel", 3, 1),
+        ("proj", 0, 1), ("dall", 1), ("trel", 3, 0), ("ddiag", 3, 0), ("ddiag", 3, 1), ("trel", 2, 3), ("sum", 1, 0),
+        ("proj", 1, 1), ("trel", 3, 1), ("trel", 3, 2), ("sum", 1, 1), ("hid", 3), ("drel", 2, 0), ("dall", 3),
+        ("proj", 0, 3), ("proj", 1, 3), ("sum", 3, 0), ("drel", 2, 1), ("proj", 3, 3), ("hid", 0), ("proj", 1, 0),
+        ("trel", 2, 1), ("ddiag", 2, 0), ("sum", 3, 3), ("sum", 3, 1), ("trel", 2, 0), ("ddiag", 2, 1), ("hid", 2),
+        ("proj", 3, 2), ("proj", 0, 2), ("sum", 2, 3), ("dall", 2), ("proj", 2, 3), ("sum", 3, 2), ("sum", 2, 0),
+        ("proj", 1, 2), ("proj", 3, 1), ("proj", 2, 1), ("proj", 2, 2), ("proj", 0, 0), ("sum", 2, 1), ("sum", 2, 2),
+        ("sum", 1, 2), ("sum", 1, 3), ("proj", 3, 0), ("sum", 0, 3), ("proj", 2, 0), ("sum", 0, 2), ("sum", 0, 1),
+        ("sum", 0, 0),
     ],
     1: [
-        ("uown",), ("usend", 3, 1), ("usend", 0, 0), ("usend", 3, 0), ("usend", 2, 1), ("norm",), ("tsend", 1, -1),
-        ("down_own",), ("urel", 3, 1), ("trel", 0, 0), ("usend", 0, 1), ("urel", 0, 0), ("udiag", 1, 1),
-        ("urel", 2, 1), ("dsend", 0, 1), ("dsend", 0, 0), ("udiag", 3, 1), ("udiag", 1, 0), ("tsend", 0, -1),
-        ("ddiag", 1, 1), ("trel", 0, 3), ("tsend", 3, 1), ("trel", 3, 0), ("urel", 0, 1), ("usend", 2, 0),
-        ("ddiag", 1, 0), ("trel", 2, 3), ("tsend", 3, 0), ("drel", 0, 1), ("tsend", 3, -1), ("drel", 0, 0),
-        ("udiag", 0, 0), ("trel", 3, 3), ("trel", 0, 1), ("urel", 3, 0), ("trel", 0, 2), ("udiag", 0, 1),
-        ("urel", 2, 0), ("tsend", 2, -1), ("tsend", 1, 1), ("trel", 3, 1), ("tsend", 0, 1), ("dsend", 3, 1),
-        ("udiag", 3, 0), ("drel", 3, 1), ("udiag", 2, 0), ("udiag", 2, 1), ("ddiag", 0, 0), ("trel", 3, 2),
-        ("dsend", 3, 0), ("tsend", 1, 0), ("uall", 1), ("ddiag", 0, 1), ("tsend", 2, 1), ("trel", 2, 0),
-        ("tsend", 0, 0), ("uall", 2), ("uall", 3), ("dall", 1), ("drel", 3, 0), ("trel", 2, 1), ("uall", 0),
-        ("dsend", 2, 1), ("tsend", 2, 0), ("hid", 3), ("hid", 0), ("dall", 0), ("ddiag", 3, 0), ("proj", 0, 0),
-        ("ddiag", 3, 1), ("dsend", 2, 0), ("proj", 0, 3), ("proj", 1, 3), ("trel", 2, 2), ("hid", 1), ("dall", 3),
-        ("drel", 2, 1), ("proj", 0, 1), ("sum", 3, 0), ("proj", 3, 3), ("drel", 2, 0), ("sum", 3, 1), ("hid", 2),
-        ("proj", 3, 0), ("sum", 3, 3), ("ddiag", 2, 0), ("ddiag", 2, 1), ("sum", 0, 3), ("proj", 3, 2),
-        ("proj", 1, 2), ("proj", 0, 2), ("sum", 0, 0), ("sum", 2, 3), ("dall", 2), ("proj", 2, 0), ("proj", 1, 0),
-        ("proj", 2, 3), ("sum", 2, 0), ("sum", 0, 2), ("proj", 2, 2), ("sum", 3, 2), ("sum", 2, 2), ("proj", 1, 1),
-        ("proj", 2, 1), ("proj", 3, 1), ("sum", 0, 1), ("sum", 2, 1), ("sum", 1, 0), ("sum", 1, 3), ("sum", 1, 1),
-        ("sum", 1, 2),
+        ("usend", 0, 1), ("uown",), ("usend", 0, 0), ("usend", 2, 1), ("norm",), ("usend", 3, 0), ("tsend", 3, -1),
+        ("down_own",), ("tsend", 2, -1), ("usend", 3, 1), ("usend", 2, 0), ("urel", 2, 1), ("dsend", 0, 0),
+        ("drel", 0, 1), ("tsend", 1, -1), ("tsend", 3, 0), ("tsend", 2, 1), ("trel", 0, 3), ("dsend", 0, 1),
+        ("urel", 2, 0), ("udiag", 1, 1), ("drel", 3, 0), ("trel", 0, 1), ("urel", 0, 1), ("trel", 2, 2),
+        ("udiag", 1, 0), ("urel", 3, 1), ("urel", 0, 0), ("tsend", 3, 1), ("tsend", 0, 0), ("urel", 3, 0),
+        ("trel", 3, 3), ("trel", 0, 2), ("udiag", 2, 1), ("tsend", 0, -1), ("ddiag", 1, 0), ("trel", 3, 1),
+        ("trel", 2, 3), ("trel", 0, 0), ("tsend", 0, 1), ("udiag", 0, 1), ("tsend", 1, 1), ("udiag", 3, 1),
+        ("udiag", 3, 0), ("drel", 3, 1), ("udiag", 2, 0), ("udiag", 0, 0), ("tsend", 1, 0), ("uall", 1),
+        ("dsend", 3, 0), ("dsend", 3, 1), ("uall", 3), ("trel", 3, 2), ("drel", 0, 0), ("trel", 3, 0),
+        ("ddiag", 1, 1), ("ddiag", 3, 0), ("uall", 0), ("ddiag", 3, 1), ("tsend", 2, 0), ("dsend", 2, 0),
+        ("dsend", 2, 1), ("uall", 2), ("hid", 1), ("dall", 1), ("trel", 2, 1), ("trel", 2, 0), ("ddiag", 0, 1),
+        ("ddiag", 0, 0), ("hid", 3), ("hid", 2), ("proj", 1, 3), ("dall", 0), ("dall", 3), ("drel", 2, 0),
+        ("proj", 0, 3), ("proj", 0, 2), ("proj", 1, 1), ("drel", 2, 1), ("sum", 3, 0), ("proj", 3, 3), ("hid", 0),
+        ("proj", 0, 0), ("proj", 1, 2), ("sum", 3, 3), ("proj", 3, 0), ("proj", 0, 1), ("ddiag", 2, 0),
+        ("ddiag", 2, 1), ("proj", 3, 1), ("proj", 3, 2), ("sum", 0, 3), ("sum", 3, 1), ("sum", 2, 3), ("sum", 0, 0),
+        ("dall", 2), ("proj", 1, 0), ("proj", 2, 3), ("sum", 3, 2), ("sum", 2, 0), ("proj", 2, 2), ("proj", 2, 1),
+        ("sum", 0, 1), ("proj", 2, 0), ("sum", 1, 0), ("sum", 2, 1), ("sum", 0, 2), ("sum", 2, 2), ("sum", 1, 2),
+        ("sum", 1, 1), ("sum", 1, 3),
     ],
 }
 
 
 def kernel(Z, X, Y, C, tok, gain, up, down, out,
-           tokb, upb, downb, tokg, upg, downg, hid, part, cin, zin, zout,
+           tokb, gainb, upb, downb, tokg, upg, downg, hid, part, cin, zin, zout,
            in_s, wz_s, wx_s, wy_s, wd_s, t_s, tc_s, rc_s, rz_s,
            wz_r, wx_r, wy_r, all_r, t_r, tc_r, rc_r, rz_r):
     T, D = tok.shape
@@ -109,29 +109,31 @@
         pltpu.make_async_copy(up, upb, in_s.at[0]),
         pltpu.make_async_copy(up.at[:, rows(z * B, B)], upg.at[y, rows(fs * Dl, Dl)], in_s.at[1]),
         pltpu.make_async_copy(tok, tokb, in_s.at[2]),
+        pltpu.make_async_copy(gain, gainb, in_s.at[5]),
         pltpu.make_async_copy(down, downb, in_s.at[3]),
         pltpu.make_async_copy(down.at[rows(z * B, B)], downg.at[fs, rows(y * B, B)], in_s.at[4]),
     ]
-    for load in loads[:3]:
+    for load in loads[:4]:
         load.start()
     loads[0].wait()
-    for load in loads[3:]:
+    for load in loads[4:]:
         load.start()
     loads[1].wait()
     pl.semaphore_wait(barrier, len(peers))
 
     def normalize():
         loads[2].wait()
+        loads[3].wait()
         RB = 32
 
         @pl.loop(0, T // RB)
         def _(i):
             v = tokb[rows(i * RB, RB), :].astype(f32)
             ms = jnp.mean(v * v, axis=-1, keepdims=True)
-            tokg[z, rows(c * T + i * RB, RB), :] = (v * lax.rsqrt(ms + epsilon) * gain[...]).astype(bf16)
-
-        loads[3].wait()
+            tokg[z, rows(c * T + i * RB, RB), :] = (v * lax.rsqrt(ms + epsilon) * gainb[...]).astype(bf16)
+
         loads[4].wait()
+        loads[5].wait()
 
     def piece(zz, xx, yy, k, half):
         f = zz * X + xx
@@ -200,8 +202,14 @@
                 h = jnp.maximum(h, 0.0)
                 hid[gg, :, rows(yy * B + j * NB, NB)] = (h * h).astype(bf16)
 
-    def sum_c(gg, f):
-        return rcopy(part.at[gg, f, oc], cin.at[gg, f], rc_s.at[0], rc_r.at[gg, f], dev(cc=oc))
+    def sum_c(g, q, f):
+        gg, zz = plane(g), plane(q)
+        return rcopy(part.at[gg, f, oc], cin.at[gg, f], rc_s.at[0], rc_r.at[gg, zz], dev(cc=oc))
+
+    def sum_c_recv(g, q):
+        gg, zz = plane(g), plane(q)
+        ref = cin.at[gg, pl.ds(zz * X, X)]
+        return rcopy(ref, ref, rc_s.at[0], rc_r.at[gg, zz], dev(cc=oc))
 
     def project(q, g):
         gg = plane(g)
@@ -212,7 +220,7 @@
             v = jnp.dot(hid[gg], downg[f], preferred_element_type=f32).astype(bf16)
             for cc in range(C):
                 part[gg, f, cc] = v[cc * T:(cc + 1) * T]
-            sum_c(gg, f).start()
+            sum_c(g, q, f).start()
 
     def sum_z(me, g, f, way, slot):
         to = jnp.where(low, z + way, z - way)
@@ -220,11 +228,11 @@
 
     def step(me, g, q):
         gg = plane(g)
+        sum_c_recv(g, q).wait_recv()
 
         @pl.loop(0, X)
         def _(xx):
             f = plane(q) * X + xx
-            sum_c(gg, f).wait_recv()
             acc = part[gg, f, c].astype(f32) + cin[gg, f].astype(f32)
             slots = ([g] if me > 0 and g >= me else []) + ([g and Z] if g <= me else [])
             for slot in slots:
@@ -327,10 +335,11 @@
         return pl.pallas_call(
             functools.partial(kernel, Z, X, Y, C),
             out_shape=jax.ShapeDtypeStruct((T, D), bf16),
-            in_specs=[hbm, vm, hbm, hbm],
+            in_specs=[hbm] * 4,
             out_specs=vm,
             scratch_shapes=[
                 pltpu.VMEM((T, D), bf16),
+                pltpu.VMEM((1, D), f32),
                 pltpu.VMEM((Dl, FFl), bf16),
                 pltpu.VMEM((FFl, Dl), bf16),
                 pltpu.VMEM((Z, C * T, D), bf16),
@@ -341,14 +350,15 @@
                 pltpu.VMEM((Z, F, T, Dl), bf16),
                 pltpu.VMEM((Z + 1, F, T, Dl), bf16),
                 pltpu.VMEM((Z, F, T, Dl), bf16),
-                dma((5,)),
+                dma((6,)),
                 *[dma((1,)) for _ in range(8)],
                 dma((2, Z, 2)), dma((2, Z)), dma((2, Z)), dma((2, Z)),
-                dma((Z, CUTS)), dma((Z,)), dma((Z, F)), dma((Z + 1, F)),
+                dma((Z, CUTS)), dma((Z,)), dma((Z, Z)), dma((Z + 1, F)),
             ],
             compiler_params=pltpu.CompilerParams(
-                collective_id=0, has_side_effects=True, vmem_limit_bytes=53 * 2**20),
-        )(tokens, norm_gain.reshape(1, D), up_weight, down_weight)
+                collective_id=0, has_side_effects=True, vmem_limit_bytes=48 * 2**20),
+        )(*[pltpu.with_memory_space_constraint(v, pltpu.HBM)
+            for v in (tokens, norm_gain.reshape(1, D), up_weight, down_weight)])
 
     return jax.shard_map(
         on_device, mesh=mesh, in_specs=placed, out_specs=P(("fs", "tp"), None), check_vma=False)

time: 102 us -> 99.9 us (0.979)
    pallas_call x1, Pallas kernels: 100 us -> 99 us  [on_device(): pl.pallas_call(functools.partial(kernel, Z, X, Y, C), out_shape=jax.Shape...]
where the time goes in v6:
time: 99.9 us; the launch traced here: 99.8 us
  Pallas kernels  99 us (99%)
    pallas_call x1, Pallas kernels, on_device(): pl.pallas_call(functools.partial(kernel, Z, X, Y, C), out_shape=jax.Shape...  99 us

profile of v6, /device:TPU:0, one launch (start us, length us, event | category | flops | bytes accessed | tf_op | source)
XLA Modules:
  0.0 99.8 jit_solution(7956912190864932775)
XLA Ops:
  0.0 99.0 %shard_map.46 = bf16[128,2048]{1,0:T(8,128)(2,1)S(1)} custom-call(bf16[128,2048]{1,0:T(8,128)(2,1)} %tok.1, f32[1,2048]{1,0:T(1,128)} %bitcast.1, bf16[256,2048]{1,0:T(8,128)(2,1)} %up.1, bf16[2048,256]{1,0:T(8,128)(2,1)} %down.1), custom_call_target="tpu_custom_call" | custom-call | tf_op jit(solution)/shard_map/pallas_call | solution.py:335
  99.0 0.8 copy.6

commit v7 on v6

--- a/solution.py
+++ b/solution.py
@@ -29,43 +29,41 @@
 
 PROGRAM = {
     0: [
-        ("uown",), ("norm",), ("usend", 2, 1), ("usend", 1, 0), ("urel", 1, 1), ("dsend", 1, 1), ("usend", 3, 1),
-        ("tsend", 3, 1), ("down_own",), ("usend", 1, 1), ("usend", 3, 0), ("urel", 2, 0), ("urel", 3, 1),
-        ("urel", 1, 0), ("dsend", 2, 0), ("tsend", 1, 1), ("udiag", 0, 1), ("udiag", 0, 0), ("usend", 2, 0),
-        ("dsend", 3, 1), ("tsend", 2, 1), ("urel", 3, 0), ("udiag", 2, 0), ("udiag", 3, 1), ("ddiag", 0, 0),
-        ("tsend", 0, 0), ("urel", 2, 1), ("udiag", 1, 1), ("dsend", 1, 0), ("drel", 1, 1), ("udiag", 1, 0),
-        ("tsend", 1, 0), ("tsend", 0, 1), ("trel", 1, 2), ("udiag", 3, 0), ("trel", 1, 1), ("udiag", 2, 1),
-        ("dsend", 3, 0), ("ddiag", 0, 1), ("drel", 1, 0), ("tsend", 2, 0), ("tsend", 3, 0), ("ddiag", 1, 1),
-        ("dsend", 2, 1), ("uall", 1), ("uall", 3), ("trel", 1, 3), ("trel", 2, 2), ("uall", 2), ("trel", 1, 0),
-        ("drel", 3, 0), ("uall", 0), ("trel", 3, 3), ("dall", 0), ("ddiag", 1, 0), ("hid", 1), ("drel", 3, 1),
-        ("proj", 0, 1), ("dall", 1), ("trel", 3, 0), ("ddiag", 3, 0), ("ddiag", 3, 1), ("trel", 2, 3), ("sum", 1, 0),
-        ("proj", 1, 1), ("trel", 3, 1), ("trel", 3, 2), ("sum", 1, 1), ("hid", 3), ("drel", 2, 0), ("dall", 3),
-        ("proj", 0, 3), ("proj", 1, 3), ("sum", 3, 0), ("drel", 2, 1), ("proj", 3, 3), ("hid", 0), ("proj", 1, 0),
-        ("trel", 2, 1), ("ddiag", 2, 0), ("sum", 3, 3), ("sum", 3, 1), ("trel", 2, 0), ("ddiag", 2, 1), ("hid", 2),
-        ("proj", 3, 2), ("proj", 0, 2), ("sum", 2, 3), ("dall", 2), ("proj", 2, 3), ("sum", 3, 2), ("sum", 2, 0),
-        ("proj", 1, 2), ("proj", 3, 1), ("proj", 2, 1), ("proj", 2, 2), ("proj", 0, 0), ("sum", 2, 1), ("sum", 2, 2),
-        ("sum", 1, 2), ("sum", 1, 3), ("proj", 3, 0), ("sum", 0, 3), ("proj", 2, 0), ("sum", 0, 2), ("sum", 0, 1),
-        ("sum", 0, 0),
+        ("uown",), ("usend", 3, 0), ("norm",), ("usend", 1, 1), ("dsend", 2, 0), ("tsend", 1, 1), ("down_own",),
+        ("tsend", 0, 1), ("dsend", 1, 0), ("udiag", 0, 1), ("urel", 1, 1), ("drel", 1, 1), ("udiag", 1, 1),
+        ("udiag", 0, 0), ("tsend", 2, 1), ("usend", 3, 1), ("ddiag", 0, 0), ("tsend", 2, 0), ("urel", 2, 1),
+        ("trel", 1, 1), ("usend", 2, 0), ("urel", 3, 0), ("tsend", 3, 1), ("urel", 2, 0), ("drel", 1, 0), ("uall", 0),
+        ("trel", 1, 2), ("urel", 3, 1), ("dsend", 1, 1), ("trel", 1, 0), ("usend", 1, 0), ("urel", 1, 0),
+        ("ddiag", 0, 1), ("ddiag", 1, 1), ("trel", 3, 0), ("ddiag", 1, 0), ("usend", 2, 1), ("udiag", 1, 0),
+        ("udiag", 3, 1), ("dsend", 2, 1), ("trel", 3, 2), ("dsend", 3, 0), ("tsend", 0, 0), ("udiag", 3, 0),
+        ("uall", 1), ("udiag", 2, 1), ("dsend", 3, 1), ("udiag", 2, 0), ("trel", 1, 3), ("dall", 0), ("drel", 3, 1),
+        ("drel", 3, 0), ("trel", 3, 1), ("trel", 3, 3), ("uall", 2), ("dall", 1), ("tsend", 3, 0), ("uall", 3),
+        ("hid", 1), ("proj", 0, 1), ("hid", 3), ("proj", 1, 3), ("tsend", 1, 0), ("sum", 1, 0), ("proj", 0, 3),
+        ("ddiag", 3, 0), ("ddiag", 3, 1), ("sum", 3, 1), ("trel", 2, 3), ("hid", 0), ("proj", 0, 0), ("dall", 3),
+        ("sum", 3, 0), ("proj", 3, 3), ("trel", 2, 1), ("proj", 3, 1), ("trel", 2, 0), ("sum", 3, 3), ("trel", 2, 2),
+        ("drel", 2, 1), ("sum", 1, 3), ("hid", 2), ("proj", 3, 2), ("proj", 1, 1), ("drel", 2, 0), ("proj", 0, 2),
+        ("sum", 2, 3), ("proj", 1, 2), ("sum", 2, 0), ("ddiag", 2, 0), ("ddiag", 2, 1), ("sum", 2, 1), ("dall", 2),
+        ("proj", 2, 3), ("sum", 3, 2), ("proj", 2, 2), ("sum", 2, 2), ("proj", 2, 1), ("proj", 3, 0), ("sum", 0, 3),
+        ("sum", 1, 2), ("proj", 1, 0), ("sum", 1, 1), ("sum", 0, 0), ("proj", 2, 0), ("sum", 0, 1), ("sum", 0, 2),
     ],
     1: [
-        ("usend", 0, 1), ("uown",), ("usend", 0, 0), ("usend", 2, 1), ("norm",), ("usend", 3, 0), ("tsend", 3, -1),
-        ("down_own",), ("tsend", 2, -1), ("usend", 3, 1), ("usend", 2, 0), ("urel", 2, 1), ("dsend", 0, 0),
-        ("drel", 0, 1), ("tsend", 1, -1), ("tsend", 3, 0), ("tsend", 2, 1), ("trel", 0, 3), ("dsend", 0, 1),
-        ("urel", 2, 0), ("udiag", 1, 1), ("drel", 3, 0), ("trel", 0, 1), ("urel", 0, 1), ("trel", 2, 2),
-        ("udiag", 1, 0), ("urel", 3, 1), ("urel", 0, 0), ("tsend", 3, 1), ("tsend", 0, 0), ("urel", 3, 0),
-        ("trel", 3, 3), ("trel", 0, 2), ("udiag", 2, 1), ("tsend", 0, -1), ("ddiag", 1, 0), ("trel", 3, 1),
-        ("trel", 2, 3), ("trel", 0, 0), ("tsend", 0, 1), ("udiag", 0, 1), ("tsend", 1, 1), ("udiag", 3, 1),
-        ("udiag", 3, 0), ("drel", 3, 1), ("udiag", 2, 0), ("udiag", 0, 0), ("tsend", 1, 0), ("uall", 1),
-        ("dsend", 3, 0), ("dsend", 3, 1), ("uall", 3), ("trel", 3, 2), ("drel", 0, 0), ("trel", 3, 0),
-        ("ddiag", 1, 1), ("ddiag", 3, 0), ("uall", 0), ("ddiag", 3, 1), ("tsend", 2, 0), ("dsend", 2, 0),
-        ("dsend", 2, 1), ("uall", 2), ("hid", 1), ("dall", 1), ("trel", 2, 1), ("trel", 2, 0), ("ddiag", 0, 1),
-        ("ddiag", 0, 0), ("hid", 3), ("hid", 2), ("proj", 1, 3), ("dall", 0), ("dall", 3), ("drel", 2, 0),
-        ("proj", 0, 3), ("proj", 0, 2), ("proj", 1, 1), ("drel", 2, 1), ("sum", 3, 0), ("proj", 3, 3), ("hid", 0),
-        ("proj", 0, 0), ("proj", 1, 2), ("sum", 3, 3), ("proj", 3, 0), ("proj", 0, 1), ("ddiag", 2, 0),
-        ("ddiag", 2, 1), ("proj", 3, 1), ("proj", 3, 2), ("sum", 0, 3), ("sum", 3, 1), ("sum", 2, 3), ("sum", 0, 0),
-        ("dall", 2), ("proj", 1, 0), ("proj", 2, 3), ("sum", 3, 2), ("sum", 2, 0), ("proj", 2, 2), ("proj", 2, 1),
-        ("sum", 0, 1), ("proj", 2, 0), ("sum", 1, 0), ("sum", 2, 1), ("sum", 0, 2), ("sum", 2, 2), ("sum", 1, 2),
-        ("sum", 1, 1), ("sum", 1, 3),
+        ("uown",), ("usend", 2, 0), ("norm",), ("usend", 0, 1), ("dsend", 0, 1), ("tsend", 1, -1), ("usend", 2, 1),
+        ("down_own",), ("usend", 3, 0), ("tsend", 0, -1), ("ddiag", 1, 0), ("urel", 2, 1), ("drel", 3, 0),
+        ("urel", 0, 1), ("tsend", 1, 0), ("udiag", 1, 1), ("usend", 3, 1), ("trel", 0, 0), ("tsend", 2, -1),
+        ("dsend", 0, 0), ("ddiag", 3, 0), ("trel", 0, 2), ("urel", 2, 0), ("tsend", 3, 0), ("usend", 0, 0),
+        ("tsend", 0, 0), ("trel", 0, 1), ("trel", 3, 0), ("ddiag", 1, 1), ("tsend", 2, 1), ("udiag", 1, 0),
+        ("trel", 0, 3), ("urel", 3, 0), ("trel", 3, 1), ("drel", 0, 1), ("tsend", 2, 0), ("tsend", 3, -1),
+        ("udiag", 3, 0), ("tsend", 3, 1), ("urel", 0, 0), ("trel", 3, 2), ("trel", 3, 3), ("urel", 3, 1),
+        ("tsend", 0, 1), ("tsend", 1, 1), ("udiag", 2, 1), ("uall", 1), ("drel", 3, 1), ("udiag", 3, 1),
+        ("trel", 2, 2), ("drel", 0, 0), ("udiag", 2, 0), ("udiag", 0, 1), ("dsend", 2, 0), ("trel", 2, 3),
+        ("trel", 2, 0), ("ddiag", 0, 1), ("dsend", 2, 1), ("udiag", 0, 0), ("dsend", 3, 1), ("trel", 2, 1),
+        ("ddiag", 0, 0), ("uall", 0), ("uall", 3), ("dall", 1), ("uall", 2), ("hid", 3), ("proj", 1, 3), ("dall", 0),
+        ("ddiag", 3, 1), ("drel", 2, 0), ("dsend", 3, 0), ("proj", 0, 3), ("hid", 1), ("drel", 2, 1), ("dall", 3),
+        ("sum", 3, 0), ("proj", 3, 1), ("proj", 3, 3), ("hid", 0), ("ddiag", 2, 1), ("proj", 1, 0), ("proj", 3, 0),
+        ("ddiag", 2, 0), ("hid", 2), ("proj", 3, 2), ("sum", 3, 3), ("sum", 3, 1), ("proj", 0, 2), ("sum", 0, 3),
+        ("sum", 2, 3), ("dall", 2), ("proj", 2, 1), ("proj", 0, 1), ("proj", 2, 0), ("proj", 2, 2), ("proj", 0, 0),
+        ("proj", 1, 1), ("sum", 2, 0), ("sum", 0, 0), ("sum", 0, 2), ("proj", 2, 3), ("sum", 1, 0), ("sum", 3, 2),
+        ("sum", 1, 3), ("proj", 1, 2), ("sum", 2, 1), ("sum", 2, 2), ("sum", 0, 1), ("sum", 1, 2), ("sum", 1, 1),
     ],
 }
 
@@ -111,7 +109,7 @@
         pltpu.make_async_copy(tok, tokb, in_s.at[2]),
         pltpu.make_async_copy(gain, gainb, in_s.at[5]),
         pltpu.make_async_copy(down, downb, in_s.at[3]),
-        pltpu.make_async_copy(down.at[rows(z * B, B)], downg.at[fs, rows(y * B, B)], in_s.at[4]),
+        pltpu.make_async_copy(down.at[rows(z * B, B)], downg.at[z, rows(y * B, B), rows(x * Dl, Dl)], in_s.at[4]),
     ]
     for load in loads[:4]:
         load.start()
@@ -139,7 +137,7 @@
         f = zz * X + xx
         if k == 0:
             return upg.at[yy, rows(f * Dl + half * (Dl // 2), Dl // 2)]
-        return downg.at[f, rows(yy * B + half * (B // 2), B // 2)]
+        return downg.at[zz, rows(yy * B + half * (B // 2), B // 2), rows(xx * Dl, Dl)]
 
     def own_piece(zz, k, half):
         if k == 0:
@@ -176,7 +174,7 @@
 
     def rest_recv(q, k):
         zz = plane(q)
-        ref = upg.at[y, pl.ds(0, 2 * Dl)] if k == 0 else downg.at[zz * X]
+        ref = upg.at[y, pl.ds(0, 2 * Dl)] if k == 0 else downg.at[zz, :, pl.ds(0, Dl)]
         return rcopy(ref, ref, wd_s.at[0], all_r.at[k, zz], dev(yy=oy))
 
     TC = T // CUTS
@@ -212,15 +210,12 @@
         return rcopy(ref, ref, rc_s.at[0], rc_r.at[gg, zz], dev(cc=oc))
 
     def project(q, g):
-        gg = plane(g)
-
-        @pl.loop(0, X)
-        def _(xx):
-            f = plane(q) * X + xx
-            v = jnp.dot(hid[gg], downg[f], preferred_element_type=f32).astype(bf16)
+        gg, zz = plane(g), plane(q)
+        v = jnp.dot(hid[gg], downg[zz], preferred_element_type=f32).astype(bf16)
+        for xx in range(X):
             for cc in range(C):
-                part[gg, f, cc] = v[cc * T:(cc + 1) * T]
-            sum_c(g, q, f).start()
+                part[gg, zz * X + xx, cc] = v[cc * T:(cc + 1) * T, xx * Dl:(xx + 1) * Dl]
+            sum_c(g, q, zz * X + xx).start()
 
     def sum_z(me, g, f, way, slot):
         to = jnp.where(low, z + way, z - way)
@@ -344,7 +339,7 @@
                 pltpu.VMEM((FFl, Dl), bf16),
                 pltpu.VMEM((Z, C * T, D), bf16),
                 pltpu.VMEM((Y, D, B), bf16),
-                pltpu.VMEM((F, Y * B, Dl), bf16),
+                pltpu.VMEM((Z, Y * B, X * Dl), bf16),
                 pltpu.VMEM((Z, C * T, Y * B), bf16),
                 pltpu.VMEM((Z, F, C, T, Dl), bf16),
                 pltpu.VMEM((Z, F, T, Dl), bf16),

time: 99.9 us -> 100 us (level)
  no operation moved by 1% of the time
where the time goes in v7:
time: 100 us
  Pallas kernels  99.2 us (99%)
    pallas_call x1, Pallas kernels, on_device(): pl.pallas_call(functools.partial(kernel, Z, X, Y, C), out_shape=jax.Shape...  99.2 us

profile of v7, /device:TPU:0, one launch (start us, length us, event | category | flops | bytes accessed | tf_op | source)
XLA Modules:
  0.0 100.1 jit_solution(5753909996634633854)
XLA Ops:
  0.0 99.2 %shard_map.46 = bf16[128,2048]{1,0:T(8,128)(2,1)S(1)} custom-call(bf16[128,2048]{1,0:T(8,128)(2,1)} %tok.1, f32[1,2048]{1,0:T(1,128)} %bitcast.1, bf16[256,2048]{1,0:T(8,128)(2,1)} %up.1, bf16[2048,256]{1,0:T(8,128)(2,1)} %down.1), custom_call_target="tpu_custom_call" | custom-call | tf_op jit(solution)/shard_map/pallas_call | solution.py:330
  99.3 0.8 copy.6
